TPU v7x, 32 devices: a whole 2x2x4 slice. The times are simulated.
32 devices in a mesh: ep: 8 (over z, x), tp: 4 (over y, core).
Axes of the slice: x: 2, y: 2, z: 4, core: 2. Of those that a mesh axis runs over, the one named last changes fastest.
Arguments:
- glu_value: bfloat16 [32768, 1024], P(('ep', 'tp')), may hold values from -6 to 6
- glu_gate: bfloat16 [32768, 1024], P(('ep', 'tp')), may hold values from -6 to 6
- conv_taps: float32 [31, 1024], replicated, may hold values from -12 to 12
- chan_gain: float32 [1024], replicated, may hold values from 0.1 to 1.9
- chan_shift: float32 [1024], replicated, may hold values from -3 to 3
- mix_out_weight: bfloat16 [1024, 2048], P('tp'), may hold values from -0.1875 to 0.1875
- moe_input: bfloat16 [4096, 2048], P(('ep', 'tp')), may hold values from -6 to 6
- moe_gain: float32 [2048], replicated, may hold values from 0.1 to 1.9
- expert_ids: int32 [4096, 4], P(('ep', 'tp')), may hold values from 0 to 31, all different within a row; in each aligned block of 128 rows (0 to 127, 128 to 255, ...) at most 20 rows name the same one
- expert_share: float32 [4096, 4], P(('ep', 'tp')), may hold values from 0.05 to 1
- expert_gate_weight: bfloat16 [32, 2048, 1024], P(('ep', 'tp')), may hold values from -0.375 to 0.375
- expert_up_weight: bfloat16 [32, 2048, 1024], P(('ep', 'tp')), may hold values from -0.375 to 0.375
- expert_down_weight: bfloat16 [32, 1024, 2048], P(('ep', 'tp')), may hold values from -0.0390625 to 0.0390625
Outputs:
- mixed: bfloat16 [32768, 2048], P(('ep', 'tp'))
- moe_output: bfloat16 [4096, 2048], P(('ep', 'tp'))
Inputs may be any that keep to these rules, and one draw needn't show every extreme that they name: `expert_ids`: each row names 4 different experts. In each aligned block of 128 rows (the rows of one device) no expert is named by more than 20 rows, and in some block one expert is named by exactly 20 rows.
All inputs are finite; a program needn't handle non-finite values.
Results may differ from a plain program's by a relative error of at most 0.0071.
Values may be sent and summed in bfloat16 or wider, within the bound.
A program may use at most 192 MiB of HBM per device.

v0:
```python
import functools

import jax
import jax.numpy as jnp
from jax import lax
from jax.experimental import pallas as pl
from jax.experimental.pallas import tpu as pltpu
from jax.sharding import PartitionSpec as P

CLAMP_LIMIT = 7.0
GLU_SLOPE = 1.702
LANES = 128
PACK = 16
MESH = pl.DeviceIdType.MESH
F32 = jnp.float32
BF16 = jnp.bfloat16


def place(flat, tp):
    return (flat // tp, flat % tp)


def greet(n, tp, me):
    barrier = pltpu.get_barrier_semaphore()

    @pl.loop(1, n)
    def _(k):
        pl.semaphore_signal(
            barrier, inc=1, device_id=place((me + k) % n, tp), device_id_type=MESH
        )

    pl.semaphore_wait(barrier, n - 1)


def slab(ref, index):
    return ref.at[pl.ds(pl.multiple_of(index * PACK, PACK), PACK)]


def exchange_copy(src, dst, ssem, rsem, me, n, tp, k):
    return pltpu.make_async_remote_copy(
        src_ref=slab(src, (me + k) % n),
        dst_ref=slab(dst, me),
        send_sem=ssem.at[k],
        recv_sem=rsem.at[k],
        device_id=place((me + k) % n, tp),
        device_id_type=MESH,
    )


def arrival(src, dst, ssem, rsem, me, n, tp, k):
    return pltpu.make_async_remote_copy(
        src_ref=slab(src, (me + k) % n),
        dst_ref=slab(dst, (me + n - k) % n),
        send_sem=ssem.at[k],
        recv_sem=rsem.at[k],
        device_id=place((me + k) % n, tp),
        device_id_type=MESH,
    )


def start_exchange(pairs, me, n, tp):
    @pl.loop(0, n - 1)
    def _(j):
        k = 1 + (j + n // 4 - 1) % (n - 1)
        for src, dst, ssem, rsem in pairs:
            exchange_copy(src, dst, ssem, rsem, me, n, tp, k).start()

    for src, dst, ssem, rsem in pairs:
        pltpu.make_async_copy(slab(src, me), slab(dst, me), ssem.at[0]).start()


def finish_exchange(pairs, me, n, tp):
    for src, dst, ssem, rsem in pairs:
        pltpu.make_async_copy(slab(src, me), slab(dst, me), ssem.at[0]).wait()

    @pl.loop(1, n)
    def _(k):
        for src, dst, ssem, rsem in pairs:
            copy = arrival(src, dst, ssem, rsem, me, n, tp, k)
            copy.wait_recv()
            copy.wait_send()


def first_kernel(
    n,
    tp,
    taps_count,
    margin,
    main,
    rest,
    value_all,
    gate_all,
    value,
    gate,
    taps,
    gain,
    shift,
    weight,
    main_out,
    rest_out,
    weight_out,
    act,
    halo_v,
    halo_g,
    glu,
    conv,
    main_s,
    main_r,
    rest_s,
    rest_r,
    halo_s,
    halo_r,
    weight_s,
    weight_r,
):
    step = pl.program_id(0)
    steps = pl.num_programs(0)
    e = lax.axis_index("ep")
    t = lax.axis_index("tp")
    me = e * tp + t
    rows, width = value.shape
    blocks = width // LANES
    depth = weight.shape[0]
    pairs = ((main, main_out, main_s, main_r), (rest, rest_out, rest_s, rest_r))
    positions = value_all.shape[0]

    def halo_copy(which, dest):
        src, dst = ((value_all, halo_v), (gate_all, halo_g))[which]
        return pltpu.make_async_remote_copy(
            src_ref=src.at[pl.ds(positions - margin, margin)],
            dst_ref=dst,
            send_sem=halo_s.at[which],
            recv_sem=halo_r.at[which],
            device_id=place(dest, tp),
            device_id_type=MESH,
        )

    sibling = t + 1 - 2 * (t % 2)

    def weight_rows(owner):
        return weight_out.at[pl.ds(pl.multiple_of(owner * depth, depth), depth)]

    def weight_copy(src, owner, dest, k):
        return pltpu.make_async_remote_copy(
            src_ref=src,
            dst_ref=weight_rows(owner),
            send_sem=weight_s.at[k],
            recv_sem=weight_r.at[k],
            device_id=(e, dest),
            device_id_type=MESH,
        )

    def weight_far(k, owner):
        return weight_copy(weight, owner, (t + k) % tp, k)

    def weight_relay(k):
        owner = (t + tp - k) % tp
        return weight_copy(weight_rows(owner), owner, sibling, k + 1)

    def weight_relayed(k):
        return weight_copy(weight, (sibling + tp - k) % tp, sibling, k + 1)

    def own_weight():
        return pltpu.make_async_copy(
            weight,
            weight_out.at[pl.ds(pl.multiple_of(t * depth, depth), depth)],
            weight_s.at[0],
        )

    @pl.when(step == 0)
    def _():
        greet(n, tp, me)

        @pl.when(me < n - 1)
        def _():
            for which in range(2):
                halo_copy(which, me + 1).start()

        for k in range(2, tp, 2):
            weight_far(k, t).start()
        weight_copy(weight, t, sibling, 1).start()
        start_exchange(pairs, me, n, tp)
        own_weight().start()

        @pl.when(me > 0)
        def _():
            for which in range(2):
                halo_copy(which, me - 1).wait_recv()
            for b in range(blocks):
                cols = slice(b * LANES, (b + 1) * LANES)
                glu[b, 0:margin, :] = halo_v[:, cols].astype(F32) * jax.nn.sigmoid(
                    halo_g[:, cols].astype(F32)
                )

        @pl.when(me == 0)
        def _():
            for b in range(blocks):
                glu[b, 0:margin, :] = jnp.zeros((margin, LANES), F32)

    @pl.when(step > 0)
    def _():
        for b in range(blocks):
            glu[b, 0:margin, :] = glu[b, rows : rows + margin, :]

    for b in range(blocks):
        cols = slice(b * LANES, (b + 1) * LANES)
        glu[b, margin : margin + rows, :] = value[:, cols].astype(F32) * jax.nn.sigmoid(
            gate[:, cols].astype(F32)
        )

    @pl.when(step == steps - 1)
    def _():
        for k in range(2, tp, 2):
            weight_far(k, (t + tp - k) % tp).wait_recv()
            weight_relay(k).start()

    part = 64
    lead = margin - (taps_count - 1)

    @pl.loop(0, rows // part)
    def _(r):
        base = r * part
        for b in range(blocks):
            cols = slice(b * LANES, (b + 1) * LANES)
            total = jnp.zeros((part, LANES), F32)
            for j in range(taps_count):
                total = total + taps[j : j + 1, cols] * glu[b, pl.ds(base + lead + j, part), :]
            conv[pl.ds(pl.multiple_of(base, part), part), cols] = total

    norm_part = 32

    @pl.loop(0, rows // norm_part)
    def _(r):
        rows_here = pl.ds(pl.multiple_of(r * norm_part, norm_part), norm_part)
        data = conv[rows_here, :]
        center = jnp.mean(data, axis=-1, keepdims=True)
        data = data - center
        spread = jnp.mean(data * data, axis=-1, keepdims=True)
        normed = data * lax.rsqrt(spread + 1e-05) * gain[...] + shift[...]
        act[rows_here, :] = (normed * jax.nn.sigmoid(normed)).astype(BF16)

    @pl.when(step == steps - 1)
    def _():
        @pl.when(me < n - 1)
        def _():
            for which in range(2):
                halo_copy(which, me + 1).wait_send()

        own_weight().wait()
        weight_copy(weight, sibling, sibling, 1).wait_recv()
        weight_copy(weight, t, sibling, 1).wait_send()
        for k in range(2, tp, 2):
            weight_far(k, t).wait_send()
            weight_relayed(k).wait_recv()
            weight_relay(k).wait_send()
        finish_exchange(pairs, me, n, tp)


def expert_kernel(
    has_main, n, spare, cuts, main, rest, gate, up, down, main_out, rest_out, rows, total
):
    step = pl.program_id(0)
    slots = n * PACK
    count = n * spare
    piece = main_out.shape[1] // cuts if has_main else total.shape[1] // cuts
    first = slots if has_main else 0
    bits = spare.bit_length() - 1

    def home(shape, dim, q):
        row = lax.broadcasted_iota(jnp.int32, shape, dim)
        slot = lax.broadcasted_iota(jnp.int32, shape, 1 - dim)
        where = (row >> bits) * PACK + (row & (spare - 1)) + q * spare
        return (where == slot).astype(F32).astype(BF16)

    @pl.when(step == 0)
    def _():
        if has_main:
            rows[0:slots, :] = main[...]
        for q in range(cuts):
            rows[first : first + count, q * piece : (q + 1) * piece] = jnp.dot(
                home((count, slots), 0, q), rest[...], preferred_element_type=F32
            ).astype(BF16)

    data = rows[...]
    pre_gate = jnp.dot(data, gate[0], preferred_element_type=F32)
    pre_up = jnp.dot(data, up[0], preferred_element_type=F32)
    gated = jnp.minimum(pre_gate, CLAMP_LIMIT)
    lifted = jnp.clip(pre_up, -CLAMP_LIMIT, CLAMP_LIMIT) + 1.0
    hidden = (lifted * gated * jax.nn.sigmoid(GLU_SLOPE * gated)).astype(BF16)
    part = jnp.dot(hidden, down[0], preferred_element_type=F32)

    @pl.when(step == 0)
    def _():
        total[...] = part

    @pl.when(step > 0)
    def _():
        total[...] += part

    @pl.when(step == pl.num_programs(0) - 1)
    def _():
        if has_main:
            main_out[...] = total[0:slots, :].astype(BF16)
        else:
            main_out[...] = main[...]
        folded = jnp.zeros(rest.shape, F32)
        for q in range(cuts):
            folded = folded + jnp.dot(
                home((slots, count), 1, q),
                total[first : first + count, q * piece : (q + 1) * piece].astype(BF16),
                preferred_element_type=F32,
            )
        rest_out[...] = folded.astype(BF16)


def second_kernel(
    n, tp, main, rest, act, weight, main_out, rest_out, mixed, main_s, main_r, rest_s, rest_r
):
    step = pl.program_id(0)
    steps = pl.num_programs(0)
    me = lax.axis_index("ep") * tp + lax.axis_index("tp")
    pairs = ((main, main_out, main_s, main_r), (rest, rest_out, rest_s, rest_r))

    @pl.when(step == 0)
    def _():
        greet(n, tp, me)
        start_exchange(pairs, me, n, tp)

    mixed[...] = jnp.dot(act[...], weight[...], preferred_element_type=F32).astype(BF16)

    @pl.when(step == steps - 1)
    def _():
        finish_exchange(pairs, me, n, tp)


def fill(block):
    return pl.BlockSpec(block, lambda i: (0,) * len(block))


ANY = pl.BlockSpec(memory_space=pl.ANY)


def body(
    n,
    tp,
    glu_value,
    glu_gate,
    conv_taps,
    chan_gain,
    chan_shift,
    mix_out_weight,
    moe_input,
    moe_gain,
    expert_ids,
    expert_share,
    expert_gate_weight,
    expert_up_weight,
    expert_down_weight,
):
    tokens, per_token = expert_ids.shape
    copies = tokens * per_token
    width = moe_input.shape[1]
    capacity = max(2, 5 * copies // (4 * n))
    spare = 1
    while spare < capacity - PACK or (capacity < PACK and spare < capacity):
        spare *= 2
    has_main = capacity >= PACK
    base = PACK if has_main else 0
    cuts = PACK // spare
    piece = width // cuts
    slots = n * PACK

    features = moe_input.astype(F32)
    scaled = features * lax.rsqrt(jnp.mean(jnp.square(features), axis=-1, keepdims=True) + 1e-06)
    moe_normed = (scaled * moe_gain).astype(BF16)

    named = jnp.sum(
        (expert_ids[:, :, None] == jnp.arange(n, dtype=jnp.int32)).astype(BF16), axis=1
    )
    below = (
        jnp.arange(tokens)[:, None] > jnp.arange(tokens)[None, :]
    ).astype(BF16)
    before = jnp.dot(below, named, preferred_element_type=F32)
    hits = [
        (expert_ids[:, k : k + 1] == jnp.arange(n, dtype=jnp.int32)).astype(F32)
        for k in range(per_token)
    ]
    rank = [jnp.sum(before * hit, axis=1, keepdims=True).astype(jnp.int32) for hit in hits]
    main_code = [
        jnp.where(rank[k] < base, expert_ids[:, k : k + 1] * PACK + rank[k], -1)
        for k in range(per_token)
    ]
    rest_code = [
        jnp.where(rank[k] >= base, expert_ids[:, k : k + 1] * PACK + rank[k] - base, -slots)
        for k in range(per_token)
    ]
    lanes = jnp.arange(slots, dtype=jnp.int32)[None, :]

    def spread(codes, scales):
        total = jnp.zeros((tokens, slots), F32)
        for k in range(per_token):
            total = total + jnp.where(codes[k] == lanes, scales[k], 0.0)
        return total

    ones = [jnp.ones((tokens, 1), F32)] * per_token
    high = lax.reduce_precision(expert_share, 8, 7)
    low = expert_share - high
    highs = [high[:, k : k + 1] for k in range(per_token)]
    lows = [low[:, k : k + 1] for k in range(per_token)]

    def pick(matrix, data):
        return lax.dot_general(
            matrix, data, (((0,), (0,)), ((), ())), preferred_element_type=F32
        ).astype(BF16)

    def pieces(data):
        return jnp.concatenate([data[:, q * piece : (q + 1) * piece] for q in range(cuts)], axis=0)

    def rest_place(scales):
        return [
            spread([code + q * spare for code in rest_code], scales).astype(BF16)
            for q in range(cuts)
        ]

    if has_main:
        main = pick(spread(main_code, ones).astype(BF16), moe_normed)
    else:
        main = jnp.zeros((slots, LANES), BF16)
    rest = pick(jnp.concatenate(rest_place(ones), axis=0), pieces(moe_normed))

    positions, channels = glu_value.shape
    taps_count = conv_taps.shape[0]
    margin = -(-(taps_count - 1) // PACK) * PACK
    tile = min(256, positions)
    steps = positions // tile
    dma = pltpu.SemaphoreType.DMA
    row_tile = pl.BlockSpec((tile, channels), lambda i: (i, 0))
    out_width = mix_out_weight.shape[1]
    main_in, rest_in, weight, act = pl.pallas_call(
        functools.partial(first_kernel, n, tp, taps_count, margin),
        grid=(steps,),
        name="dispatch_and_conv",
        out_shape=(
            jax.ShapeDtypeStruct(main.shape, BF16),
            jax.ShapeDtypeStruct(rest.shape, BF16),
            jax.ShapeDtypeStruct((channels, out_width), BF16),
            jax.ShapeDtypeStruct((positions, channels), BF16),
        ),
        in_specs=[
            ANY,
            ANY,
            ANY,
            ANY,
            row_tile,
            row_tile,
            fill(conv_taps.shape),
            fill((1, channels)),
            fill((1, channels)),
            pl.BlockSpec(memory_space=pltpu.VMEM),
        ],
        out_specs=(ANY, ANY, ANY, row_tile),
        scratch_shapes=[
            pltpu.VMEM((margin, channels), BF16),
            pltpu.VMEM((margin, channels), BF16),
            pltpu.VMEM((channels // LANES, margin + tile, LANES), F32),
            pltpu.VMEM((tile, channels), F32),
            dma((n,)),
            dma((n,)),
            dma((n,)),
            dma((n,)),
            dma((2,)),
            dma((2,)),
            dma((tp,)),
            dma((tp,)),
        ],
        compiler_params=pltpu.CompilerParams(
            collective_id=0,
            has_side_effects=True,
            dimension_semantics=("arbitrary",),
            vmem_limit_bytes=32 * 1024 * 1024,
        ),
    )(
        main,
        rest,
        glu_value,
        glu_gate,
        glu_value,
        glu_gate,
        conv_taps,
        chan_gain.reshape(1, channels),
        chan_shift.reshape(1, channels),
        mix_out_weight,
    )

    hidden_units = expert_gate_weight.shape[2]
    block = min(256, hidden_units)
    count = (slots if has_main else 0) + n * spare
    columns = pl.BlockSpec((1, width, block), lambda f: (0, 0, f))
    main_answers, rest_answers = pl.pallas_call(
        functools.partial(expert_kernel, has_main, n, spare, cuts),
        grid=(hidden_units // block,),
        name="experts",
        out_shape=(
            jax.ShapeDtypeStruct(main.shape, BF16),
            jax.ShapeDtypeStruct(rest.shape, BF16),
        ),
        in_specs=[
            fill(main.shape),
            fill(rest.shape),
            columns,
            columns,
            pl.BlockSpec((1, block, width), lambda f: (0, f, 0)),
        ],
        out_specs=(fill(main.shape), fill(rest.shape)),
        scratch_shapes=[pltpu.VMEM((count, width), BF16), pltpu.VMEM((count, width), F32)],
        compiler_params=pltpu.CompilerParams(
            dimension_semantics=("arbitrary",), vmem_limit_bytes=44 * 1024 * 1024
        ),
    )(main_in, rest_in, expert_gate_weight, expert_up_weight, expert_down_weight)

    main_back, rest_back, mixed = pl.pallas_call(
        functools.partial(second_kernel, n, tp),
        grid=(steps,),
        name="return_and_mix",
        out_shape=(
            jax.ShapeDtypeStruct(main.shape, BF16),
            jax.ShapeDtypeStruct(rest.shape, BF16),
            jax.ShapeDtypeStruct((positions, out_width), BF16),
        ),
        in_specs=[ANY, ANY, row_tile, fill((channels, out_width))],
        out_specs=(ANY, ANY, pl.BlockSpec((tile, out_width), lambda i: (i, 0))),
        scratch_shapes=[dma((n,)), dma((n,)), dma((n,)), dma((n,))],
        compiler_params=pltpu.CompilerParams(
            collective_id=1,
            has_side_effects=True,
            dimension_semantics=("arbitrary",),
            vmem_limit_bytes=32 * 1024 * 1024,
        ),
    )(main_answers, rest_answers, act, weight)

    def weigh(parts, data):
        both = jnp.dot(jnp.concatenate(parts, axis=0), data, preferred_element_type=F32)
        return both[:tokens] + both[tokens:]

    highs_rest, lows_rest = rest_place(highs), rest_place(lows)
    combined = jnp.concatenate(
        [weigh([highs_rest[q], lows_rest[q]], rest_back) for q in range(cuts)], axis=1
    )
    if has_main:
        combined = combined + weigh(
            [spread(main_code, highs).astype(BF16), spread(main_code, lows).astype(BF16)],
            main_back,
        )
    return (mixed, combined.astype(BF16))


def solution(mesh):
    tp = mesh.shape["tp"]
    n = mesh.shape["ep"] * tp
    both = P(("ep", "tp"), None)
    weights = P(("ep", "tp"), None, None)
    placed = (
        both, both, P(), P(), P(), P("tp", None), both, P(), both, both, weights, weights, weights
    )
    return jax.shard_map(
        functools.partial(body, n, tp),
        mesh=mesh,
        in_specs=placed,
        out_specs=(both, both),
        check_vma=False,
    )
```

profile of v0, /device:TPU:15, one launch (start us, length us, event | category | flops | bytes accessed | tf_op | source)
XLA Modules:
  0.0 160.7 jit_solution(11303066304859223852)
XLA Ops:
  0.6 0.8 slice_bitcast_fusion.10
  1.5 0.7 fusion.47
  2.2 0.2 select_reduce_fusion.3
  2.4 0.8 add_bitcast_fusion.11
  3.2 0.7 fusion.61
  3.9 0.6 add_convert_fusion.5
  4.5 0.6 add_convert_fusion.9
  5.1 0.2 fusion
  5.3 0.2 fusion.2
  5.6 0.0 copy-start.1
  5.6 0.0 copy-start.3
  5.6 0.5 convolution_convert_fusion.1.rest
  6.1 0.0 copy-start
  6.1 0.0 copy-start.4
  6.1 0.0 copy-start.5
  6.1 0.0 copy-start.6
  6.1 0.9 convolution_convert_fusion.main
  7.0 0.2 copy-done.1
  7.2 0.3 copy-done.3
  7.4 0.8 copy-done
  8.2 0.0 copy-done.5
  8.2 68.0 %dispatch_and_conv.1 = (bf16[512,2048]{1,0:T(8,128)(2,1)S(1)}, bf16[512,512]{1,0:T(8,128)(2,1)S(1)}, bf16[1024,2048]{1,0:T(8,128)(2,1)S(1)}, bf16[1024,1024]{1,0:T(8,128)(2,1)S(1)}) custom-call(bf16[512,2048]{1,0:T(8,128)(2,1)S(1)} %convolution_convert_fusion.main, bf16[512,512]{1,0:T(8,128)(2,1)S(1)} %convolution_convert_fusion.1.rest, ...), custom_call_target="tpu_custom_call" | custom-call | tf_op jit(solution)/shard_map/dispatch_and_conv/pallas_call | solution.py:439
  76.3 14.2 %experts.1 = (bf16[512,2048]{1,0:T(8,128)(2,1)S(1)}, bf16[512,512]{1,0:T(8,128)(2,1)S(1)}) custom-call(bf16[512,2048]{1,0:T(8,128)(2,1)S(1)} %get-tuple-element.11.main, bf16[512,512]{1,0:T(8,128)(2,1)S(1)} %get-tuple-element.12.rest, bf16[1,2048,1024]{2,1,0:T(8,128)(2,1)S(1)} %copy-done.2, bf16[1,2048,1024]{2,1,0:T(8,128)(2,1)} %up.1, ...), custom_call_target="tpu_custom_call" | custom-call | tf_op jit(solution)/shard_map/experts/pallas_call | solution.py:499
  90.5 64.8 %return_and_mix.1 = (bf16[512,2048]{1,0:T(8,128)(2,1)S(1)}, bf16[512,512]{1,0:T(8,128)(2,1)S(1)}, bf16[1024,2048]{1,0:T(8,128)(2,1)S(1)}) custom-call(bf16[512,2048]{1,0:T(8,128)(2,1)S(1)} %get-tuple-element.13.main, bf16[512,512]{1,0:T(8,128)(2,1)S(1)} %get-tuple-element.14.rest, bf16[1024,1024]{1,0:T(8,128)(2,1)S(1)} %get-tuple-element.15.act, ...), custom_call_target="tpu_custom_call" | custom-call | tf_op jit(solution)/shard_map/return_and_mix/pallas_call | solution.py:521
  155.3 0.3 fusion.31
  155.7 0.3 fusion.27
  156.0 0.3 fusion.23
  156.4 0.3 fusion.19
  156.7 0.3 add_convert_fusion.1
  157.0 0.7 fusion.35
  157.7 1.0 fusion.4
  158.7 2.0 %copy.17 = bf16[1024,2048]{1,0:T(8,128)(2,1)} copy(bf16[1024,2048]{1,0:T(8,128)(2,1)S(1)} %get-tuple-element.95) | data formatting | bytes 8388608
  (17 shorter events, 0.2 us)
Async XLA Ops:
  0.6 4.5 %copy-start.7 = (bf16[128,2048]{1,0:T(8,128)(2,1)S(1)}, bf16[128,2048]{1,0:T(8,128)(2,1)}, u32[]{:S(2)}) copy-start(bf16[128,2048]{1,0:T(8,128)(2,1)} %param.19) | copy-start | bytes 1572868
  0.6 4.7 %copy-start.8 = (f32[2048]{0:T(1024)S(1)}, f32[2048]{0:T(1024)}, u32[]{:S(2)}) copy-start(f32[2048]{0:T(1024)} %param.20) | copy-start | bytes 24580
  5.6 1.6 copy-start.1
  5.6 1.8 %copy-start.3 = (bf16[256,2048]{1,0:T(8,128)(2,1)S(1)}, bf16[256,2048]{1,0:T(8,128)(2,1)}, u32[]{:S(2)}) copy-start(bf16[256,2048]{1,0:T(8,128)(2,1)} %weight.1) | copy-start | bytes 3145732
  6.1 2.2 %copy-start = (bf16[1024,1024]{1,0:T(8,128)(2,1)S(1)}, bf16[1024,1024]{1,0:T(8,128)(2,1)}, u32[]{:S(2)}) copy-start(bf16[1024,1024]{1,0:T(8,128)(2,1)} %value.1) | copy-start | bytes 6291460
  6.1 2.2 %copy-start.4 = (f32[31,1024]{1,0:T(8,128)S(1)}, f32[31,1024]{1,0:T(8,128)}, u32[]{:S(2)}) copy-start(f32[31,1024]{1,0:T(8,128)} %taps.1) | copy-start | bytes 380932
  6.1 2.2 %copy-start.5 = (f32[1024]{0:T(1024)S(1)}, f32[1024]{0:T(1024)}, u32[]{:S(2)}) copy-start(f32[1024]{0:T(1024)} %param.16) | copy-start | bytes 12292
  6.1 2.1 %copy-start.6 = (f32[1024]{0:T(1024)S(1)}, f32[1024]{0:T(1024)}, u32[]{:S(2)}) copy-start(f32[1024]{0:T(1024)} %param.17) | copy-start | bytes 12292
  8.2 68.0 %copy-start.2 = (bf16[1,2048,1024]{2,1,0:T(8,128)(2,1)S(1)}, bf16[1,2048,1024]{2,1,0:T(8,128)(2,1)}, u32[]{:S(2)}) copy-start(bf16[1,2048,1024]{2,1,0:T(8,128)(2,1)} %gate.3) | copy-start | bytes 12582916
where the time goes:
time: 161 us
  Pallas kernels  147 us (91%)
  other arithmetic  5.2 us (3%)
  local copies, waits for them, and re-layouts  4.18 us (3%)
  matrix products  3.39 us (2%)
    pallas_call x1, Pallas kernels, body(): pl.pallas_call(functools.partial(first_kernel, n, tp, taps_count, margin)...  68 us
    pallas_call x1, Pallas kernels, body(): pl.pallas_call(functools.partial(second_kernel, n, tp), grid=(steps,), na...  64.8 us
    pallas_call x1, Pallas kernels, body(): pl.pallas_call(functools.partial(expert_kernel, has_main, n, spare, cuts)...  14.2 us
    unnamed x19, local copies, waits for them, and re-layouts  3.3 us

commit v1 on v0

v1 whole, which is shorter than its diff:
```python
import functools

import jax
import jax.numpy as jnp
from jax import lax
from jax.experimental import pallas as pl
from jax.experimental.pallas import tpu as pltpu
from jax.sharding import PartitionSpec as P

CLAMP_LIMIT = 7.0
GLU_SLOPE = 1.702
LANES = 128
PACK = 16
CUT = 2
KINDS = 4
MESH = pl.DeviceIdType.MESH
F32 = jnp.float32
BF16 = jnp.bfloat16


def place(flat, tp):
    return (flat // tp, flat % tp)


def rows_of(index, size):
    return pl.ds(pl.multiple_of(index * size, size), size)


def visit_order(depth):
    table = []
    for z in range(depth):
        near = sorted(range(depth), key=lambda other: (abs(other - z), other))
        table.append(near)
    return table


def source_at(depth, z, slot):
    table = visit_order(depth)
    picked = 0
    for a in range(depth):
        for b in range(depth):
            picked = picked + jnp.where((z == a) & (slot == b), table[a][b], 0)
    return picked


def remote(src, dst, ssem, rsem, flat, tp):
    return pltpu.make_async_remote_copy(
        src_ref=src,
        dst_ref=dst,
        send_sem=ssem,
        recv_sem=rsem,
        device_id=place(flat, tp),
        device_id_type=MESH,
    )


def greet(n, tp, slab, me, with_next):
    barrier = pltpu.get_barrier_semaphore()
    z, s = me // slab, me % slab
    depth = n // slab

    def hail(flat):
        pl.semaphore_signal(barrier, inc=1, device_id=place(flat, tp), device_id_type=MESH)

    @pl.loop(1, slab)
    def _(k):
        hail(z * slab + (s + k) % slab)

    edges = [(z < depth - 1, slab), (z > 0, -slab)]
    if with_next:
        edges.append(((s == slab - 1) & (z < depth - 1), 1))
        edges.append(((s == 0) & (z > 0), -1))
    total = slab - 1
    for there, step in edges:

        @pl.when(there)
        def _():
            hail(me + step)

        total = total + jnp.where(there, 1, 0)
    pl.semaphore_wait(barrier, total)


class Shape:
    def __init__(self, n, tp, tokens, per_token, width):
        slab = tp * max(1, tp // 2)
        while n % slab:
            slab //= 2
        self.n, self.tp, self.slab, self.depth = n, tp, slab, n // slab
        self.tokens, self.width = tokens, width
        copies = tokens * per_token
        capacity = max(2, 5 * copies // (4 * n))
        self.has_main = capacity >= PACK
        spare = 1
        while spare < capacity - PACK or (capacity < PACK and spare < capacity):
            spare *= 2
        self.spare = spare
        self.bits = spare.bit_length() - 1
        self.cuts = PACK // spare
        self.base = PACK if self.has_main else 0
        self.w = width // CUT
        self.main_w = self.w if self.has_main else 0
        self.piece = self.w // self.cuts
        self.block_w = self.main_w + self.piece
        self.pack_w = CUT * self.block_w
        self.slots = slab * PACK
        self.first = self.slots if self.has_main else 0
        self.count = self.first + slab * spare
        self.table_rows = -(-self.depth * KINDS // 8) * 8


def first_kernel(
    sh,
    taps_count,
    margin,
    tok,
    tab,
    value_all,
    gate_all,
    taps,
    gain,
    shift,
    weight,
    wg,
    wu,
    wd,
    answers,
    tabs_out,
    weight_out,
    act_out,
    held,
    tabs,
    packs,
    takes,
    data,
    hidden,
    total,
    reply,
    wg_v,
    wu_v,
    wd_v,
    value,
    gate,
    halo_v,
    halo_g,
    glu,
    conv,
    act,
    z_r,
    up_s,
    down_s,
    slab_s,
    slab_r,
    halo_s,
    halo_r,
    weight_s,
    weight_r,
    load_s,
    store_s,
):
    n, tp, slab, depth = sh.n, sh.tp, sh.slab, sh.depth
    e = lax.axis_index("ep")
    t = lax.axis_index("tp")
    me = e * tp + t
    z, s = me // slab, me % slab
    positions, channels = value.shape
    blocks = channels // LANES
    shard = weight.shape[0]
    chunk = shard // depth

    loads = [
        pltpu.make_async_copy(value_all, value, load_s.at[0]),
        pltpu.make_async_copy(gate_all, gate, load_s.at[1]),
        pltpu.make_async_copy(wg.at[0], wg_v, load_s.at[2]),
        pltpu.make_async_copy(wu.at[0], wu_v, load_s.at[3]),
        pltpu.make_async_copy(wd.at[0], wd_v, load_s.at[4]),
    ]
    for load in loads:
        load.start()

    def line_copy(part, src, own, up):
        if part < CUT:
            cols = slice(part * sh.w, (part + 1) * sh.w)
            there = held.at[src, :, cols]
            here = tok.at[:, cols] if own else there
        else:
            there = tabs.at[src]
            here = tab if own else there
        sems = up_s if up else down_s
        return remote(
            here, there, sems.at[src, part], z_r.at[src, part], me + (slab if up else -slab), tp
        )

    def halo_copy(which, dest):
        src, dst = ((value_all, halo_v), (gate_all, halo_g))[which]
        return remote(
            src.at[pl.ds(positions - margin, margin)],
            dst,
            halo_s.at[which],
            halo_r.at[which],
            dest,
            tp,
        )

    sibling = t + 1 - 2 * (t % 2)

    def weight_part(owner, c):
        start = pl.multiple_of(owner * shard + c * chunk, chunk)
        return weight_out.at[pl.ds(start, chunk)]

    def weight_copy(src, owner, c, dest, k):
        return remote(
            src, weight_part(owner, c), weight_s.at[k, c], weight_r.at[k, c], e * tp + dest, tp
        )

    def weight_own(c):
        return weight.at[rows_of(c, chunk)]

    def weight_far(k, owner, c):
        return weight_copy(weight_own(c), owner, c, (t + k) % tp, k)

    def weight_relay(k, c):
        owner = (t + tp - k) % tp
        return weight_copy(weight_part(owner, c), owner, c, sibling, k + 1)

    def weight_relayed(k, c):
        return weight_copy(weight_own(c), (sibling + tp - k) % tp, c, sibling, k + 1)

    def own_weight():
        return pltpu.make_async_copy(
            weight, weight_out.at[rows_of(t, shard)], store_s.at[0]
        )

    def block_copy(slot, h, k, sender, owner):
        cols = slice(h * sh.block_w, (h + 1) * sh.block_w)
        return remote(
            packs.at[slot, rows_of((s + k) % slab, PACK), cols],
            takes.at[slot, rows_of(sender, PACK), cols],
            slab_s.at[slot, h, k],
            slab_r.at[slot, h, k],
            z * slab + owner,
            tp,
        )

    def reply_copy(slot):
        return pltpu.make_async_copy(reply.at[slot], answers.at[slot], store_s.at[1 + slot])

    tile = positions // depth

    def act_copy(c):
        return pltpu.make_async_copy(
            act.at[rows_of(c, tile)], act_out.at[rows_of(c, tile)], store_s.at[1 + depth + c]
        )

    held[z] = tok[...]
    tabs[z] = tab[...]
    greet(n, tp, slab, me, True)

    for part in (CUT, *range(CUT)):

        @pl.when(z < depth - 1)
        def _():
            line_copy(part, z, True, True).start()

        @pl.when(z > 0)
        def _():
            line_copy(part, z, True, False).start()

    @pl.when(me < n - 1)
    def _():
        for which in range(2):
            halo_copy(which, me + 1).start()

    @pl.loop(0, depth)
    def _(c):
        weight_copy(weight_own(c), t, c, sibling, 1).start()

    own_weight().start()

    def pack_rows(slot, h, src):
        cols = h * sh.w
        token = lax.broadcasted_iota(jnp.int32, (sh.tokens, sh.slots), 0).astype(F32) + 1.0
        lane = lax.broadcasted_iota(jnp.int32, (sh.tokens, sh.slots), 1)
        at = h * sh.block_w

        def gathered(mask, lo, size):
            return lax.dot_general(
                mask.astype(F32).astype(BF16),
                held[src, :, lo : lo + size],
                (((0,), (0,)), ((), ())),
                preferred_element_type=F32,
            )

        if sh.has_main:
            named = tabs[src, pl.ds(z * KINDS, 1), :]
            packs[slot, :, at : at + sh.w] = gathered(named == token, cols, sh.w).astype(BF16)
        spare_named = tabs[src, pl.ds(z * KINDS + 2, 1), :]
        hit = spare_named == token
        part = (lane >> sh.bits) & (sh.cuts - 1)
        folded = jnp.zeros((sh.slots, sh.piece), F32)
        for q in range(sh.cuts):
            folded = folded + gathered(hit & (part == q), cols + q * sh.piece, sh.piece)
        packs[slot, :, at + sh.main_w : at + sh.block_w] = folded.astype(BF16)

    def home(shape, dim, q):
        row = lax.broadcasted_iota(jnp.int32, shape, dim)
        slot = lax.broadcasted_iota(jnp.int32, shape, 1 - dim)
        where = (row >> sh.bits) * PACK + (row & (sh.spare - 1)) + q * sh.spare
        return (where == slot).astype(F32).astype(BF16)

    spare_rows = slab * sh.spare
    hidden_units = wg_v.shape[1]
    block = min(256, hidden_units)

    def experts(slot):
        for h in range(CUT):
            at = h * sh.block_w
            if sh.has_main:
                data[0 : sh.slots, h * sh.w : (h + 1) * sh.w] = takes[slot, :, at : at + sh.w]
            rest = takes[slot, :, at + sh.main_w : at + sh.block_w]
            for q in range(sh.cuts):
                lo = h * sh.w + q * sh.piece
                data[sh.first : sh.count, lo : lo + sh.piece] = jnp.dot(
                    home((spare_rows, sh.slots), 0, q), rest, preferred_element_type=F32
                ).astype(BF16)

        for f in range(hidden_units // block):
            cols = slice(f * block, (f + 1) * block)
            pre_gate = jnp.dot(data[...], wg_v[:, cols], preferred_element_type=F32)
            pre_up = jnp.dot(data[...], wu_v[:, cols], preferred_element_type=F32)
            gated = jnp.minimum(pre_gate, CLAMP_LIMIT)
            lifted = jnp.clip(pre_up, -CLAMP_LIMIT, CLAMP_LIMIT) + 1.0
            hidden[:, cols] = (lifted * gated * jax.nn.sigmoid(GLU_SLOPE * gated)).astype(BF16)

        step = min(512, sh.width)
        for f in range(sh.width // step):
            cols = slice(f * step, (f + 1) * step)
            total[:, cols] = jnp.dot(
                hidden[...], wd_v[:, cols], preferred_element_type=F32
            ).astype(BF16)

        for h in range(CUT):
            at = h * sh.block_w
            if sh.has_main:
                reply[slot, :, at : at + sh.w] = total[0 : sh.slots, h * sh.w : (h + 1) * sh.w]
            folded = jnp.zeros((sh.slots, sh.piece), F32)
            for q in range(sh.cuts):
                lo = h * sh.w + q * sh.piece
                folded = folded + jnp.dot(
                    home((sh.slots, spare_rows), 1, q),
                    total[sh.first : sh.count, lo : lo + sh.piece],
                    preferred_element_type=F32,
                )
            reply[slot, :, at + sh.main_w : at + sh.block_w] = folded.astype(BF16)

    part = 64
    norm_part = 32
    lead = margin - (taps_count - 1)

    def conv_tile(c):
        top = c * tile
        for b in range(blocks):
            cols = slice(b * LANES, (b + 1) * LANES)
            here = rows_of(c, tile)
            there = pl.ds(pl.multiple_of(margin + top, PACK), tile)
            glu[b, there, :] = value[here, cols].astype(F32) * jax.nn.sigmoid(
                gate[here, cols].astype(F32)
            )

        @pl.loop(0, tile // part)
        def _(r):
            base = top + r * part
            for b in range(blocks):
                cols = slice(b * LANES, (b + 1) * LANES)
                summed = jnp.zeros((part, LANES), F32)
                for j in range(taps_count):
                    summed = (
                        summed + taps[j : j + 1, cols] * glu[b, pl.ds(base + lead + j, part), :]
                    )
                conv[rows_of(r, part), cols] = summed

        @pl.loop(0, tile // norm_part)
        def _(r):
            rows = conv[rows_of(r, norm_part), :]
            center = jnp.mean(rows, axis=-1, keepdims=True)
            rows = rows - center
            spread = jnp.mean(rows * rows, axis=-1, keepdims=True)
            normed = rows * lax.rsqrt(spread + 1e-05) * gain[...] + shift[...]
            there = pl.ds(pl.multiple_of(top + r * norm_part, norm_part), norm_part)
            act[there, :] = (normed * jax.nn.sigmoid(normed)).astype(BF16)

        act_copy(c).start()

    @pl.loop(0, depth + 1)
    def _(i):
        @pl.when(i < depth)
        def _():
            src = source_at(depth, z, i)
            for part in (CUT, *range(CUT)):

                @pl.when(i > 0)
                def _():
                    line_copy(part, src, False, True).wait_recv()

                @pl.when((i > 0) & (src < z) & (z < depth - 1))
                def _():
                    line_copy(part, src, False, True).start()

                @pl.when((src > z) & (z > 0))
                def _():
                    line_copy(part, src, False, False).start()

                if part < CUT:
                    pack_rows(i, part, src)

                    @pl.loop(1, slab)
                    def _(k):
                        block_copy(i, part, k, s, (s + k) % slab).start()

            takes[i, rows_of(s, PACK), :] = packs[i, rows_of(s, PACK), :]
            for k in range(2, tp, 2):
                weight_far(k, t, i).start()

        @pl.when(i > 0)
        def _():
            for k in range(2, tp, 2):
                weight_far(k, (t + tp - k) % tp, i - 1).wait_recv()
                weight_relay(k, i - 1).start()

        @pl.when(i == 0)
        def _():
            loads[0].wait()
            loads[1].wait()

            @pl.when(me > 0)
            def _():
                for which in range(2):
                    halo_copy(which, me - 1).wait_recv()
                for b in range(blocks):
                    cols = slice(b * LANES, (b + 1) * LANES)
                    glu[b, 0:margin, :] = halo_v[:, cols].astype(F32) * jax.nn.sigmoid(
                        halo_g[:, cols].astype(F32)
                    )

            @pl.when(me == 0)
            def _():
                for b in range(blocks):
                    glu[b, 0:margin, :] = jnp.zeros((margin, LANES), F32)

        low = jnp.where(i == 0, 0, jnp.minimum(i + 1, depth))
        high = jnp.minimum(i + 2, depth)

        @pl.loop(low, high)
        def _(c):
            conv_tile(c)

        @pl.when(i == 1)
        def _():
            for load in loads[2:]:
                load.wait()

        @pl.when(i > 0)
        def _():
            for h in range(CUT):

                @pl.loop(1, slab)
                def _(k):
                    block_copy(i - 1, h, k, (s + slab - k) % slab, s).wait_recv()

            experts(i - 1)
            reply_copy(i - 1).start()

    tabs_out[...] = tabs[...]

    @pl.when(me < n - 1)
    def _():
        for which in range(2):
            halo_copy(which, me + 1).wait_send()

    own_weight().wait()

    @pl.loop(0, depth)
    def _(c):
        weight_copy(weight_own(c), sibling, c, sibling, 1).wait_recv()
        weight_copy(weight_own(c), t, c, sibling, 1).wait_send()
        for k in range(2, tp, 2):
            weight_far(k, t, c).wait_send()
            weight_relayed(k, c).wait_recv()
            weight_relay(k, c).wait_send()
        act_copy(c).wait()
        reply_copy(c).wait()
        for part in range(CUT + 1):

            @pl.when((z < depth - 1) & (c <= z))
            def _():
                line_copy(part, c, False, True).wait_send()

            @pl.when((z > 0) & (c >= z))
            def _():
                line_copy(part, c, False, False).wait_send()

        for h in range(CUT):

            @pl.loop(1, slab)
            def _(k):
                block_copy(c, h, k, s, (s + k) % slab).wait_send()


def second_kernel(
    sh,
    answers,
    tabs,
    act,
    weight,
    moe_out,
    mixed,
    back,
    come,
    away,
    sums,
    act_v,
    weight_v,
    mixed_v,
    slab_s,
    slab_r,
    line_s,
    line_r,
    load_s,
    store_s,
):
    n, tp, slab, depth = sh.n, sh.tp, sh.slab, sh.depth
    me = lax.axis_index("ep") * tp + lax.axis_index("tp")
    z, s = me // slab, me % slab
    tiles = 2 * depth
    tile = act_v.shape[0] // tiles

    loads = [
        pltpu.make_async_copy(act, act_v, load_s.at[0]),
        pltpu.make_async_copy(weight, weight_v, load_s.at[1]),
    ]

    def block_copy(slot, h, k, owner, dest):
        cols = slice(h * sh.block_w, (h + 1) * sh.block_w)
        return remote(
            answers.at[slot, rows_of((s + k) % slab, PACK), cols],
            back.at[slot, rows_of(owner, PACK), cols],
            slab_s.at[slot, h, k],
            slab_r.at[slot, h, k],
            z * slab + dest,
            tp,
        )

    def own_copy(slot):
        return pltpu.make_async_copy(
            answers.at[slot, rows_of(s, PACK)], back.at[slot, rows_of(s, PACK)], load_s.at[2 + slot]
        )

    def line_copy(h, target, index, up):
        cols = slice(h * sh.w, (h + 1) * sh.w)
        return remote(
            away.at[target, :, cols],
            come.at[index, :, cols],
            line_s.at[target, h],
            line_r.at[index, h],
            me + (slab if up else -slab),
            tp,
        )

    def mixed_copy(c):
        return pltpu.make_async_copy(
            mixed_v.at[rows_of(c, tile)], mixed.at[rows_of(c, tile)], store_s.at[c]
        )

    greet(n, tp, slab, me, False)

    @pl.loop(0, depth)
    def _(m):
        slot = depth - 1 - m
        for h in range(CUT):

            @pl.loop(1, slab)
            def _(k):
                block_copy(slot, h, k, s, (s + k) % slab).start()

        own_copy(slot).start()

    for load in loads:
        load.start()
    for load in loads:
        load.wait()

    def weights_of(source, kind):
        token = lax.broadcasted_iota(jnp.int32, (sh.tokens, sh.slots), 0).astype(F32) + 1.0
        named = tabs[source, pl.ds(z * KINDS + kind, 1), :]
        share = tabs[source, pl.ds(z * KINDS + kind + 1, 1), :]
        full = jnp.where(named == token, share, 0.0)
        high = full.astype(BF16)
        low = (full - high.astype(F32)).astype(BF16)
        return high, low

    def weigh(high, low, rows):
        return jnp.dot(high, rows, preferred_element_type=F32) + jnp.dot(
            low, rows, preferred_element_type=F32
        )

    out_step = min(512, weight_v.shape[1])

    @pl.loop(0, depth)
    def _(m):
        slot = depth - 1 - m
        target = source_at(depth, z, slot)

        @pl.loop(0, 2)
        def _(u):
            c = m * 2 + u
            for f in range(weight_v.shape[1] // out_step):
                cols = slice(f * out_step, (f + 1) * out_step)
                mixed_v[rows_of(c, tile), cols] = jnp.dot(
                    act_v[rows_of(c, tile), :], weight_v[:, cols], preferred_element_type=F32
                ).astype(BF16)
            mixed_copy(c).start()

        own_copy(slot).wait()
        lane = lax.broadcasted_iota(jnp.int32, (sh.tokens, sh.slots), 1)
        part = (lane >> sh.bits) & (sh.cuts - 1)
        for h in range(CUT):

            @pl.loop(1, slab)
            def _(k):
                block_copy(slot, h, k, (s + slab - k) % slab, s).wait_recv()

            at = h * sh.block_w
            spare_high, spare_low = weights_of(target, 2)
            rest = back[slot, :, at + sh.main_w : at + sh.block_w]
            zero = jnp.zeros_like(spare_high)
            for q in range(sh.cuts):
                sums[:, q * sh.piece : (q + 1) * sh.piece] = weigh(
                    jnp.where(part == q, spare_high, zero),
                    jnp.where(part == q, spare_low, zero),
                    rest,
                )
            if sh.has_main:
                high, low = weights_of(target, 0)
                sums[...] += weigh(high, low, back[slot, :, at : at + sh.w])

            cols = slice(h * sh.w, (h + 1) * sh.w)
            from_below = (z > 0) & (target >= z)
            from_above = (z < depth - 1) & (target < z)
            final_above = (z < depth - 1) & (target == z)

            @pl.when(from_below | from_above)
            def _():
                line_copy(h, target, target, True).wait_recv()
                sums[...] += come[target, :, cols].astype(F32)

            @pl.when(final_above)
            def _():
                line_copy(h, target, depth, True).wait_recv()
                sums[...] += come[depth, :, cols].astype(F32)

            @pl.when(target == z)
            def _():
                moe_out[:, cols] = sums[...].astype(BF16)

            @pl.when(target != z)
            def _():
                away[target, :, cols] = sums[...].astype(BF16)

            @pl.when(target > z)
            def _():
                line_copy(h, target, target, True).start()

            @pl.when(target < z)
            def _():
                index = jnp.where(target == z - 1, depth, target)
                line_copy(h, target, index, False).start()

    @pl.loop(0, depth)
    def _(c):
        for h in range(CUT):

            @pl.loop(1, slab)
            def _(k):
                block_copy(c, h, k, s, (s + k) % slab).wait_send()

            @pl.when(c != z)
            def _():
                line_copy(h, c, c, True).wait_send()

    @pl.loop(0, tiles)
    def _(c):
        mixed_copy(c).wait()


ANY = pl.BlockSpec(memory_space=pl.ANY)
VMEM = pl.BlockSpec(memory_space=pltpu.VMEM)


def route_tables(sh, expert_ids, expert_share):
    n, tokens = sh.n, sh.tokens
    experts = jnp.arange(n, dtype=jnp.int32)
    chosen = (expert_ids[:, :, None] == experts).astype(F32)
    named = jnp.sum(chosen, axis=1).astype(BF16)
    below = (jnp.arange(tokens)[:, None] > jnp.arange(tokens)[None, :]).astype(BF16)
    before = jnp.dot(below, named, preferred_element_type=F32)
    rank = jnp.sum(before[:, None, :] * chosen, axis=2).astype(jnp.int32)

    lanes = jnp.arange(n * PACK, dtype=jnp.int32)
    main_code = jnp.where(rank < sh.base, expert_ids * PACK + rank, -1)
    spare_code = jnp.where(rank >= sh.base, expert_ids * sh.spare + rank - sh.base, -1)
    spare_lane = (lanes // PACK) * sh.spare + lanes % sh.spare
    number = jnp.arange(1, tokens + 1, dtype=jnp.int32).astype(F32)[:, None, None]
    share = expert_share[:, :, None]
    main_hit = main_code[:, :, None] == lanes
    spare_hit = spare_code[:, :, None] == spare_lane
    kinds = [
        jnp.sum(jnp.where(hit, what, 0.0), axis=(0, 1))
        for hit in (main_hit, spare_hit)
        for what in (number, share)
    ]
    table = jnp.stack([kind.reshape(sh.depth, sh.slots) for kind in kinds], axis=1)
    table = table.reshape(sh.depth * KINDS, sh.slots)
    return jnp.pad(table, ((0, sh.table_rows - sh.depth * KINDS), (0, 0)))


def body(
    n,
    tp,
    glu_value,
    glu_gate,
    conv_taps,
    chan_gain,
    chan_shift,
    mix_out_weight,
    moe_input,
    moe_gain,
    expert_ids,
    expert_share,
    expert_gate_weight,
    expert_up_weight,
    expert_down_weight,
):
    tokens, per_token = expert_ids.shape
    width = moe_input.shape[1]
    sh = Shape(n, tp, tokens, per_token, width)
    slab, depth = sh.slab, sh.depth

    features = moe_input.astype(F32)
    scaled = features * lax.rsqrt(jnp.mean(jnp.square(features), axis=-1, keepdims=True) + 1e-06)
    moe_normed = (scaled * moe_gain).astype(BF16)
    table = route_tables(sh, expert_ids, expert_share)

    positions, channels = glu_value.shape
    taps_count = conv_taps.shape[0]
    margin = -(-(taps_count - 1) // PACK) * PACK
    out_width = mix_out_weight.shape[1]
    hidden_units = expert_gate_weight.shape[2]
    dma = pltpu.SemaphoreType.DMA
    packed = (depth, sh.slots, sh.pack_w)
    answers, tabs, weight, act = pl.pallas_call(
        functools.partial(first_kernel, sh, taps_count, margin),
        name="dispatch_conv_experts",
        out_shape=(
            jax.ShapeDtypeStruct(packed, BF16),
            jax.ShapeDtypeStruct((depth, *table.shape), F32),
            jax.ShapeDtypeStruct((channels, out_width), BF16),
            jax.ShapeDtypeStruct((positions, channels), BF16),
        ),
        in_specs=[VMEM, VMEM, ANY, ANY, VMEM, VMEM, VMEM, VMEM, ANY, ANY, ANY],
        out_specs=(ANY, VMEM, ANY, ANY),
        scratch_shapes=[
            pltpu.VMEM((depth, tokens, width), BF16),
            pltpu.VMEM((depth, *table.shape), F32),
            pltpu.VMEM(packed, BF16),
            pltpu.VMEM(packed, BF16),
            pltpu.VMEM((sh.count, width), BF16),
            pltpu.VMEM((sh.count, hidden_units), BF16),
            pltpu.VMEM((sh.count, width), BF16),
            pltpu.VMEM(packed, BF16),
            pltpu.VMEM((width, hidden_units), BF16),
            pltpu.VMEM((width, hidden_units), BF16),
            pltpu.VMEM((hidden_units, width), BF16),
            pltpu.VMEM((positions, channels), BF16),
            pltpu.VMEM((positions, channels), BF16),
            pltpu.VMEM((margin, channels), BF16),
            pltpu.VMEM((margin, channels), BF16),
            pltpu.VMEM((channels // LANES, margin + positions, LANES), F32),
            pltpu.VMEM((positions // depth, channels), F32),
            pltpu.VMEM((positions, channels), BF16),
            dma((depth, CUT + 1)),
            dma((depth, CUT + 1)),
            dma((depth, CUT + 1)),
            dma((depth, CUT, slab)),
            dma((depth, CUT, slab)),
            dma((2,)),
            dma((2,)),
            dma((tp, depth)),
            dma((tp, depth)),
            dma((5,)),
            dma((1 + 2 * depth,)),
        ],
        compiler_params=pltpu.CompilerParams(
            collective_id=0, has_side_effects=True, vmem_limit_bytes=56 * 1024 * 1024
        ),
    )(
        moe_normed,
        table,
        glu_value,
        glu_gate,
        conv_taps,
        chan_gain.reshape(1, channels),
        chan_shift.reshape(1, channels),
        mix_out_weight,
        expert_gate_weight,
        expert_up_weight,
        expert_down_weight,
    )

    moe_output, mixed = pl.pallas_call(
        functools.partial(second_kernel, sh),
        name="return_and_mix",
        out_shape=(
            jax.ShapeDtypeStruct((tokens, width), BF16),
            jax.ShapeDtypeStruct((positions, out_width), BF16),
        ),
        in_specs=[ANY, VMEM, ANY, ANY],
        out_specs=(VMEM, ANY),
        scratch_shapes=[
            pltpu.VMEM(packed, BF16),
            pltpu.VMEM((depth + 1, tokens, width), BF16),
            pltpu.VMEM((depth, tokens, width), BF16),
            pltpu.VMEM((tokens, sh.w), F32),
            pltpu.VMEM((positions, channels), BF16),
            pltpu.VMEM((channels, out_width), BF16),
            pltpu.VMEM((positions, out_width), BF16),
            dma((depth, CUT, slab)),
            dma((depth, CUT, slab)),
            dma((depth, CUT)),
            dma((depth + 1, CUT)),
            dma((2 + depth,)),
            dma((2 * depth,)),
        ],
        compiler_params=pltpu.CompilerParams(
            collective_id=1, has_side_effects=True, vmem_limit_bytes=48 * 1024 * 1024
        ),
    )(answers, tabs, act, weight)
    return (mixed, moe_output)


def solution(mesh):
    tp = mesh.shape["tp"]
    n = mesh.shape["ep"] * tp
    both = P(("ep", "tp"), None)
    weights = P(("ep", "tp"), None, None)
    placed = (
        both, both, P(), P(), P(), P("tp", None), both, P(), both, both, weights, weights, weights
    )
    return jax.shard_map(
        functools.partial(body, n, tp),
        mesh=mesh,
        in_specs=placed,
        out_specs=(both, both),
        check_vma=False,
    )
```

time: 161 us -> 143 us (0.89)
  the two profiles are of different devices: /device:TPU:15 before, /device:TPU:0 now
where the time goes in v1:
time: 143 us; the launch traced here: 142 us
  Pallas kernels  124 us (87%)
  local copies, waits for them, and re-layouts  9.66 us (7%)
  other arithmetic  7.12 us (5%)
    pallas_call x1, Pallas kernels, body(): pl.pallas_call(functools.partial(first_kernel, sh, taps_count, margin), n...  74.2 us
    pallas_call x1, Pallas kernels, body(): pl.pallas_call(functools.partial(second_kernel, sh), name='return_and_mix...  50.2 us
    unnamed x8, local copies, waits for them, and re-layouts  9.66 us

profile of v1, /device:TPU:0, one launch (start us, length us, event | category | flops | bytes accessed | tf_op | source)
XLA Modules:
  0.0 142.0 jit_solution(1794262452270439046)
XLA Ops:
  0.6 1.2 fusion
  1.9 0.7 convert_reduce_fusion
  2.6 0.1 fusion.5
  2.7 0.7 select_reduce_fusion.2
  3.4 0.7 add_select_fusion.2
  4.1 1.1 fusion.3
  5.3 0.6 pad_maximum_fusion
  5.9 2.0 %fusion.2.tok = bf16[128,2048]{1,0:T(8,128)(2,1)} fusion(bf16[128,2048]{1,0:T(8,128)(2,1)} %param.19, f32[2048]{0:T(1024)} %param.20, f32[128]{0:T(128)S(1)} %add_rsqrt_fusion), kind=kLoop, calls=%fused_computation.6 | loop fusion | flops 1048576 | bytes 1057280 | tf_op jit(solution)/shard_map/convert_element_type | solution.py:750
  7.9 74.2 %dispatch_conv_experts.1 = (bf16[4,128,2560]{2,1,0:T(8,128)(2,1)}, f32[4,16,128]{2,1,0:T(8,128)}, bf16[1024,2048]{1,0:T(8,128)(2,1)}, bf16[1024,1024]{1,0:T(8,128)(2,1)}) custom-call(bf16[128,2048]{1,0:T(8,128)(2,1)} %fusion.2.tok, f32[16,128]{1,0:T(8,128)} %bitcast.8, bf16[1024,1024]{1,0:T(8,128)(2,1)} %value_all.1, bf16[1024,1024]{1,0:T(8,128)(2,1)} %gate_all.1, ...), custom_call_target="tpu_custom_call" | custom-call | tf_op jit(solution)/shard_map/dispatch_conv_experts/pallas_call | solution.py:760
  82.2 0.0 copy-start
  82.2 1.7 %copy-done = bf16[4,128,2560]{2,1,0:T(8,128)(2,1)S(1)} copy-done((bf16[4,128,2560]{2,1,0:T(8,128)(2,1)S(1)}, bf16[4,128,2560]{2,1,0:T(8,128)(2,1)}, u32[]{:S(2)}) %copy-start) | copy-done | bytes 2621464
  83.9 0.0 copy-start.1
  83.9 1.6 %copy-done.1 = bf16[1024,1024]{1,0:T(8,128)(2,1)S(1)} copy-done((bf16[1024,1024]{1,0:T(8,128)(2,1)S(1)}, bf16[1024,1024]{1,0:T(8,128)(2,1)}, u32[]{:S(2)}) %copy-start.1) | copy-done | bytes 2097176
  85.5 0.0 copy-start.2
  85.5 0.8 copy-done.2
  86.3 50.2 %return_and_mix.1 = (bf16[128,2048]{1,0:T(8,128)(2,1)S(1)}, bf16[1024,2048]{1,0:T(8,128)(2,1)}) custom-call(bf16[4,128,2560]{2,1,0:T(8,128)(2,1)S(1)} %copy-done, f32[4,16,128]{2,1,0:T(8,128)S(1)} %copy-done.2, bf16[1024,1024]{1,0:T(8,128)(2,1)S(1)} %copy-done.1, bf16[1024,2048]{1,0:T(8,128)(2,1)} %get-tuple-element.11.weight), custom_call_target="tpu_custom_call" | custom-call | tf_op jit(solution)/shard_map/return_and_mix/pallas_call | solution.py:819
  136.4 4.8 %copy.22 = bf16[1024,2048]{1,0:T(8,128)(2,1)} copy(bf16[1024,2048]{1,0:T(8,128)(2,1)} %get-tuple-element.22) | data formatting | bytes 8388608
  141.2 0.8 copy.23
  (3 shorter events, 0.0 us)
Async XLA Ops:
  82.2 1.7 %copy-start = (bf16[4,128,2560]{2,1,0:T(8,128)(2,1)S(1)}, bf16[4,128,2560]{2,1,0:T(8,128)(2,1)}, u32[]{:S(2)}) copy-start(bf16[4,128,2560]{2,1,0:T(8,128)(2,1)} %get-tuple-element.8.answers) | copy-start | bytes 7864324
  83.9 1.6 %copy-start.1 = (bf16[1024,1024]{1,0:T(8,128)(2,1)S(1)}, bf16[1024,1024]{1,0:T(8,128)(2,1)}, u32[]{:S(2)}) copy-start(bf16[1024,1024]{1,0:T(8,128)(2,1)} %get-tuple-element.10.act) | copy-start | bytes 6291460
  85.5 0.8 copy-start.2

commit v2 on v1

v2 whole, which is shorter than its diff:
```python
import functools

import jax
import jax.numpy as jnp
from jax import lax
from jax.experimental import pallas as pl
from jax.experimental.pallas import tpu as pltpu
from jax.sharding import PartitionSpec as P

CLAMP_LIMIT = 7.0
GLU_SLOPE = 1.702
LANES = 128
PACK = 16
CUT = 2
HOP = 4
KINDS = 4
FEED = 2
MESH = pl.DeviceIdType.MESH
F32 = jnp.float32
BF16 = jnp.bfloat16


def place(flat, tp):
    return (flat // tp, flat % tp)


def rows_of(index, size):
    return pl.ds(pl.multiple_of(index * size, size), size)


def visit_order(depth):
    table = []
    for z in range(depth):
        near = sorted(range(depth), key=lambda other: (abs(other - z), other))
        table.append(near)
    return table


def drain_order(depth):
    table = []
    for z in range(depth):
        upward = [(z + k, z + k) for k in range(1, depth - z)] if z > 0 else []
        downward = (
            [(depth - 1 - z + k, z - k) for k in range(1, z + 1)] if z < depth - 1 else []
        )
        events = [target for _, target in sorted(upward + downward)]
        table.append(events + [-1] * (depth - len(events)))
    return table


def looked_up(table, z, slot):
    picked = 0
    for a, row in enumerate(table):
        for b, entry in enumerate(row):
            picked = picked + jnp.where((z == a) & (slot == b), entry, 0)
    return picked


def remote(src, dst, ssem, rsem, flat, tp):
    return pltpu.make_async_remote_copy(
        src_ref=src,
        dst_ref=dst,
        send_sem=ssem,
        recv_sem=rsem,
        device_id=place(flat, tp),
        device_id_type=MESH,
    )


def greet(n, tp, slab, me, with_next):
    barrier = pltpu.get_barrier_semaphore()
    z, s = me // slab, me % slab
    depth = n // slab

    def hail(flat):
        pl.semaphore_signal(barrier, inc=1, device_id=place(flat, tp), device_id_type=MESH)

    @pl.loop(1, slab)
    def _(k):
        hail(z * slab + (s + k) % slab)

    edges = [(z < depth - 1, slab), (z > 0, -slab)]
    if with_next:
        edges.append(((s == slab - 1) & (z < depth - 1), 1))
        edges.append(((s == 0) & (z > 0), -1))
    total = slab - 1
    for there, step in edges:

        @pl.when(there)
        def _():
            hail(me + step)

        total = total + jnp.where(there, 1, 0)
    return total


class Shape:
    def __init__(self, n, tp, tokens, per_token, width):
        slab = tp * max(1, tp // 2)
        while n % slab:
            slab //= 2
        self.n, self.tp, self.slab, self.depth = n, tp, slab, n // slab
        self.tokens, self.width = tokens, width
        copies = tokens * per_token
        capacity = max(2, 5 * copies // (4 * n))
        self.has_main = capacity >= PACK
        spare = 1
        while spare < capacity - PACK or (capacity < PACK and spare < capacity):
            spare *= 2
        self.spare = spare
        self.bits = spare.bit_length() - 1
        self.cuts = PACK // spare
        self.base = PACK if self.has_main else 0
        self.w = width // CUT
        self.main_w = self.w if self.has_main else 0
        self.piece = self.w // self.cuts
        self.block_w = self.main_w + self.piece
        self.pack_w = CUT * self.block_w
        self.slots = slab * PACK
        self.first = self.slots if self.has_main else 0
        self.count = self.first + slab * spare
        self.table_rows = -(-self.depth * KINDS // 8) * 8


def prepare(sh, features_ref, gain, id_rows, share_rows, normed, table):
    n, tokens = sh.n, sh.tokens
    features = features_ref[...].astype(F32)
    scale = lax.rsqrt(jnp.mean(features * features, axis=-1, keepdims=True) + 1e-06)
    normed[...] = (features * scale * gain[...]).astype(BF16)

    def upright(rows):
        rows = rows[...].astype(F32)
        blank = jnp.zeros((8 - rows.shape[0] % 8, tokens), F32)
        return jnp.transpose(jnp.concatenate([rows, blank], axis=0))

    ids = upright(id_rows).astype(jnp.int32)
    share = upright(share_rows)
    expert = lax.broadcasted_iota(jnp.int32, (tokens, n), 1)
    hits = [(ids[:, k : k + 1] == expert).astype(F32) for k in range(id_rows.shape[0])]
    named = hits[0]
    for hit in hits[1:]:
        named = named + hit
    below = (
        lax.broadcasted_iota(jnp.int32, (tokens, tokens), 0)
        > lax.broadcasted_iota(jnp.int32, (tokens, tokens), 1)
    )
    before = jnp.dot(
        below.astype(F32).astype(BF16), named.astype(BF16), preferred_element_type=F32
    )
    number = lax.broadcasted_iota(jnp.int32, (tokens, sh.slots), 0).astype(F32) + 1.0
    lane = lax.broadcasted_iota(jnp.int32, (tokens, sh.slots), 1)
    main_lane = lane
    spare_lane = lane // PACK * sh.spare + lane % sh.spare
    codes = []
    for k, hit in enumerate(hits):
        chosen = ids[:, k : k + 1]
        rank = jnp.sum(before * hit, axis=1, keepdims=True).astype(jnp.int32)
        main_code = jnp.where(rank < sh.base, chosen * PACK + rank, -1)
        spare_code = jnp.where(rank >= sh.base, chosen * sh.spare + rank - sh.base, -1)
        codes.append((main_code, spare_code, share[:, k : k + 1]))
    table[...] = jnp.zeros_like(table)
    for z in range(sh.depth):
        for kind, lanes, start in (
            (0, main_lane, z * sh.slots),
            (1, spare_lane, z * sh.slab * sh.spare),
        ):
            names = jnp.zeros((tokens, sh.slots), F32)
            shares = jnp.zeros((tokens, sh.slots), F32)
            for code in codes:
                hit = code[kind] - start == lanes
                names = names + jnp.where(hit, number, 0.0)
                shares = shares + jnp.where(hit, code[2], 0.0)
            row = z * KINDS + 2 * kind
            table[row : row + 1, :] = jnp.sum(names, axis=0, keepdims=True)
            table[row + 1 : row + 2, :] = jnp.sum(shares, axis=0, keepdims=True)


def whole_kernel(
    sh,
    taps_count,
    margin,
    moe,
    moe_gain,
    id_rows,
    share_rows,
    value_all,
    gate_all,
    taps,
    gain,
    shift,
    weight,
    wg,
    wu,
    wd,
    mixed,
    moe_out,
    held,
    tabs,
    packs,
    takes,
    data,
    hidden,
    total,
    reply,
    back,
    come,
    away,
    parts,
    wg_v,
    wu_v,
    wd_v,
    weight_v,
    value,
    gate,
    halo_v,
    halo_g,
    glu,
    conv,
    act,
    z_r,
    up_s,
    down_s,
    slab_s,
    slab_r,
    back_s,
    back_r,
    line_s,
    line_r,
    halo_s,
    halo_r,
    weight_s,
    weight_r,
    cross_s,
    cross_r,
    load_s,
    moe_v,
    moe_gain_v,
    id_v,
    share_v,
    taps_v,
    gain_v,
    shift_v,
):
    n, tp, slab, depth = sh.n, sh.tp, sh.slab, sh.depth
    e = lax.axis_index("ep")
    t = lax.axis_index("tp")
    me = e * tp + t
    z, s = me // slab, me % slab
    positions, channels = value.shape
    blocks = channels // LANES
    shard = weight.shape[0]
    order = visit_order(depth)
    late = drain_order(depth)

    loads = [
        pltpu.make_async_copy(value_all, value, load_s.at[0]),
        pltpu.make_async_copy(gate_all, gate, load_s.at[1]),
        pltpu.make_async_copy(wg.at[0], wg_v, load_s.at[2]),
        pltpu.make_async_copy(wu.at[0], wu_v, load_s.at[3]),
        pltpu.make_async_copy(wd.at[0], wd_v, load_s.at[4]),
        pltpu.make_async_copy(weight, weight_v.at[rows_of(t, shard)], load_s.at[5]),
    ]
    small = [
        pltpu.make_async_copy(here, there, load_s.at[6 + at])
        for at, (here, there) in enumerate(
            (
                (moe, moe_v),
                (moe_gain, moe_gain_v),
                (id_rows, id_v),
                (share_rows, share_v),
                (taps, taps_v),
                (gain, gain_v),
                (shift, shift_v),
            )
        )
    ]
    for load in small + loads:
        load.start()

    def line_copy(part, src, up):
        if part < CUT:
            cols = slice(part * sh.w, (part + 1) * sh.w)
            there = held.at[src, :, cols]
            here = there
        else:
            there = tabs.at[src]
            here = there
        sems = up_s if up else down_s
        return remote(
            here, there, sems.at[src, part], z_r.at[src, part], me + (slab if up else -slab), tp
        )

    def halo_copy(which, dest):
        src, dst = ((value_all, halo_v), (gate_all, halo_g))[which]
        return remote(
            src.at[pl.ds(positions - margin, margin)],
            dst,
            halo_s.at[which],
            halo_r.at[which],
            dest,
            tp,
        )

    sibling = t + 1 - 2 * (t % 2)
    across = slab // tp
    halves = 2 if across % 2 == 0 else 1
    x = (me // tp) % across
    mine = x % halves
    partner = e + 1 - 2 * (x % 2)
    chunk = shard // (halves * FEED)

    def weight_rows(owner, half, c):
        start = owner * shard + (half * FEED + c) * chunk
        return weight_v.at[pl.ds(pl.multiple_of(start, chunk), chunk)]

    def weight_far(k, owner, c):
        start = pl.multiple_of((mine * FEED + c) * chunk, chunk)
        return remote(
            weight.at[pl.ds(start, chunk)],
            weight_rows(owner, mine, c),
            weight_s.at[k, c],
            weight_r.at[k, c],
            e * tp + (t + k) % tp,
            tp,
        )

    def weight_relay(k, owner, c):
        here = weight_rows(owner, mine, c)
        return remote(
            here, here, weight_s.at[k + 1, c], weight_r.at[k + 1, c], e * tp + sibling, tp
        )

    def weight_cross(k, owner, half, c):
        here = weight_rows(owner, half, c)
        return remote(here, here, cross_s.at[k, c], cross_r.at[k, c], partner * tp + t, tp)

    def cross_relay(k, owner, c):
        here = weight_rows(owner, 1 - mine, c)
        return remote(here, here, cross_s.at[k + 1, c], cross_r.at[k + 1, c], e * tp + sibling, tp)

    def weight_own(owner):
        return remote(
            weight,
            weight_v.at[rows_of(owner, shard)],
            weight_s.at[1, 0],
            weight_r.at[1, 0],
            e * tp + sibling,
            tp,
        )

    def far_owner(base, k):
        return (base + tp - k) % tp

    def block_copy(slot, h, k, sender, owner):
        cols = slice(h * sh.block_w, (h + 1) * sh.block_w)
        return remote(
            packs.at[slot, rows_of((s + k) % slab, PACK), cols],
            takes.at[slot, rows_of(sender, PACK), cols],
            slab_s.at[slot, h, k],
            slab_r.at[slot, h, k],
            z * slab + owner,
            tp,
        )

    def back_copy(slot, h, k, owner, dest):
        cols = slice(h * sh.block_w, (h + 1) * sh.block_w)
        return remote(
            reply.at[slot, rows_of((s + k) % slab, PACK), cols],
            back.at[slot, rows_of(owner, PACK), cols],
            back_s.at[slot, h, k],
            back_r.at[slot, h, k],
            z * slab + dest,
            tp,
        )

    hop_w = sh.width // HOP
    fold = HOP // CUT

    def chain_copy(p, target, index, up):
        cols = slice(p * hop_w, (p + 1) * hop_w)
        return remote(
            away.at[target, :, cols],
            come.at[index, :, cols],
            line_s.at[target, p],
            line_r.at[index, p],
            me + (slab if up else -slab),
            tp,
        )

    expected = greet(n, tp, slab, me, True)
    for load in small:
        load.wait()
    prepare(sh, moe_v, moe_gain_v, id_v, share_v, held.at[z], tabs.at[z])
    pl.semaphore_wait(pltpu.get_barrier_semaphore(), expected)

    for part in (CUT, *range(CUT)):

        @pl.when(z < depth - 1)
        def _():
            line_copy(part, z, True).start()

        @pl.when(z > 0)
        def _():
            line_copy(part, z, False).start()

    @pl.when(me < n - 1)
    def _():
        for which in range(2):
            halo_copy(which, me + 1).start()

    weight_own(t).start()

    def arrive(k, part):
        for src, there, onward, up in (
            (z - k, z >= k, z < depth - 1, True),
            (z + k, z + k < depth, z > 0, False),
        ):

            @pl.when(there)
            def _():
                line_copy(part, src, up).wait_recv()

            @pl.when(there & onward)
            def _():
                line_copy(part, src, up).start()

    def pack_rows(slot, h, src):
        cols = h * sh.w
        token = lax.broadcasted_iota(jnp.int32, (sh.tokens, sh.slots), 0).astype(F32) + 1.0
        lane = lax.broadcasted_iota(jnp.int32, (sh.tokens, sh.slots), 1)
        at = h * sh.block_w

        def gathered(mask, lo, size):
            return lax.dot_general(
                mask.astype(F32).astype(BF16),
                held[src, :, lo : lo + size],
                (((0,), (0,)), ((), ())),
                preferred_element_type=F32,
            )

        if sh.has_main:
            named = tabs[src, pl.ds(z * KINDS, 1), :]
            packs[slot, :, at : at + sh.w] = gathered(named == token, cols, sh.w).astype(BF16)
        spare_named = tabs[src, pl.ds(z * KINDS + 2, 1), :]
        hit = spare_named == token
        part = (lane >> sh.bits) & (sh.cuts - 1)
        folded = jnp.zeros((sh.slots, sh.piece), F32)
        for q in range(sh.cuts):
            folded = folded + gathered(hit & (part == q), cols + q * sh.piece, sh.piece)
        packs[slot, :, at + sh.main_w : at + sh.block_w] = folded.astype(BF16)

    def home(shape, dim, q):
        row = lax.broadcasted_iota(jnp.int32, shape, dim)
        slot = lax.broadcasted_iota(jnp.int32, shape, 1 - dim)
        where = (row >> sh.bits) * PACK + (row & (sh.spare - 1)) + q * sh.spare
        return (where == slot).astype(F32).astype(BF16)

    spare_rows = slab * sh.spare
    hidden_units = wg_v.shape[1]
    block = min(256, hidden_units)

    def experts(slot):
        for h in range(CUT):
            at = h * sh.block_w
            if sh.has_main:
                data[0 : sh.slots, h * sh.w : (h + 1) * sh.w] = takes[slot, :, at : at + sh.w]
            rest = takes[slot, :, at + sh.main_w : at + sh.block_w]
            for q in range(sh.cuts):
                lo = h * sh.w + q * sh.piece
                data[sh.first : sh.count, lo : lo + sh.piece] = jnp.dot(
                    home((spare_rows, sh.slots), 0, q), rest, preferred_element_type=F32
                ).astype(BF16)

        for f in range(hidden_units // block):
            cols = slice(f * block, (f + 1) * block)
            pre_gate = jnp.dot(data[...], wg_v[:, cols], preferred_element_type=F32)
            pre_up = jnp.dot(data[...], wu_v[:, cols], preferred_element_type=F32)
            gated = jnp.minimum(pre_gate, CLAMP_LIMIT)
            lifted = jnp.clip(pre_up, -CLAMP_LIMIT, CLAMP_LIMIT) + 1.0
            hidden[:, cols] = (lifted * gated * jax.nn.sigmoid(GLU_SLOPE * gated)).astype(BF16)

        step = min(512, sh.width)
        for f in range(sh.width // step):
            cols = slice(f * step, (f + 1) * step)
            total[:, cols] = jnp.dot(
                hidden[...], wd_v[:, cols], preferred_element_type=F32
            ).astype(BF16)

        for h in range(CUT):
            at = h * sh.block_w
            if sh.has_main:
                reply[slot, :, at : at + sh.w] = total[0 : sh.slots, h * sh.w : (h + 1) * sh.w]
            folded = jnp.zeros((sh.slots, sh.piece), F32)
            for q in range(sh.cuts):
                lo = h * sh.w + q * sh.piece
                folded = folded + jnp.dot(
                    home((sh.slots, spare_rows), 1, q),
                    total[sh.first : sh.count, lo : lo + sh.piece],
                    preferred_element_type=F32,
                )
            reply[slot, :, at + sh.main_w : at + sh.block_w] = folded.astype(BF16)

    part_rows = 64
    norm_rows = 32
    lead = margin - (taps_count - 1)
    tile = positions // depth

    def conv_tile(c):
        top = c * tile
        here = rows_of(c, tile)

        @pl.when(c > 0)
        def _():
            for b in range(blocks):
                glu[b, 0:margin, :] = glu[b, tile : tile + margin, :]

        for b in range(blocks):
            cols = slice(b * LANES, (b + 1) * LANES)
            glu[b, margin : margin + tile, :] = value[here, cols].astype(F32) * jax.nn.sigmoid(
                gate[here, cols].astype(F32)
            )

        @pl.loop(0, tile // part_rows)
        def _(r):
            base = r * part_rows
            for b in range(blocks):
                cols = slice(b * LANES, (b + 1) * LANES)
                summed = jnp.zeros((part_rows, LANES), F32)
                for j in range(taps_count):
                    summed = (
                        summed
                        + taps_v[j : j + 1, cols] * glu[b, pl.ds(base + lead + j, part_rows), :]
                    )
                conv[rows_of(r, part_rows), cols] = summed

        @pl.loop(0, tile // norm_rows)
        def _(r):
            rows = conv[rows_of(r, norm_rows), :]
            center = jnp.mean(rows, axis=-1, keepdims=True)
            rows = rows - center
            spread = jnp.mean(rows * rows, axis=-1, keepdims=True)
            normed = rows * lax.rsqrt(spread + 1e-05) * gain_v[...] + shift_v[...]
            there = pl.ds(pl.multiple_of(top + r * norm_rows, norm_rows), norm_rows)
            act[there, :] = (normed * jax.nn.sigmoid(normed)).astype(BF16)

    def weights_of(source, kind):
        token = lax.broadcasted_iota(jnp.int32, (sh.tokens, sh.slots), 0).astype(F32) + 1.0
        named = tabs[source, pl.ds(z * KINDS + kind, 1), :]
        share = tabs[source, pl.ds(z * KINDS + kind + 1, 1), :]
        full = jnp.where(named == token, share, 0.0)
        high = full.astype(BF16)
        low = (full - high.astype(F32)).astype(BF16)
        return high, low

    def weigh(high, low, rows):
        return jnp.dot(high, rows, preferred_element_type=F32) + jnp.dot(
            low, rows, preferred_element_type=F32
        )

    def pass_on(p, target):
        @pl.when(target > z)
        def _():
            chain_copy(p, target, target, True).start()

        @pl.when(target < z)
        def _():
            index = jnp.where(target == z - 1, depth, target)
            chain_copy(p, target, index, False).start()

    def combine(slot):
        target = looked_up(order, z, slot)
        begins = ((z == 0) & (target > 0)) | ((z == depth - 1) & (target < z))
        lane = lax.broadcasted_iota(jnp.int32, (sh.tokens, sh.slots), 1)
        part = (lane >> sh.bits) & (sh.cuts - 1)
        for h in range(CUT):

            @pl.loop(1, slab)
            def _(k):
                back_copy(slot, h, k, (s + slab - k) % slab, s).wait_recv()

            at = h * sh.block_w
            cols = slice(h * sh.w, (h + 1) * sh.w)
            spare_high, spare_low = weights_of(target, 2)
            rest = back[slot, :, at + sh.main_w : at + sh.block_w]
            zero = jnp.zeros_like(spare_high)
            for q in range(sh.cuts):
                lo = h * sh.w + q * sh.piece
                parts[target, :, lo : lo + sh.piece] = weigh(
                    jnp.where(part == q, spare_high, zero),
                    jnp.where(part == q, spare_low, zero),
                    rest,
                )
            if sh.has_main:
                high, low = weights_of(target, 0)
                parts[target, :, cols] += weigh(high, low, back[slot, :, at : at + sh.w])

            @pl.when(begins)
            def _():
                away[target, :, cols] = parts[target, :, cols].astype(BF16)
                for f in range(fold):
                    pass_on(h * fold + f, target)

    out_w = weight_v.shape[1]
    out_step = min(512, out_w)
    mix_rows = positions // (2 * depth)

    def mix(c):
        for f in range(out_w // out_step):
            cols = slice(f * out_step, (f + 1) * out_step)
            mixed[rows_of(c, mix_rows), cols] = jnp.dot(
                act[rows_of(c, mix_rows), :], weight_v[:, cols], preferred_element_type=F32
            ).astype(BF16)

    def dispatch(slot, h):
        pack_rows(slot, h, looked_up(order, z, slot))

        @pl.loop(1, slab)
        def _(k):
            block_copy(slot, h, k, s, (s + k) % slab).start()

        cols = slice(h * sh.block_w, (h + 1) * sh.block_w)
        takes[slot, rows_of(s, PACK), cols] = packs[slot, rows_of(s, PACK), cols]

    def send_back(slot):
        for h in range(CUT):

            @pl.loop(1, slab)
            def _(k):
                back_copy(slot, h, k, s, (s + k) % slab).start()

        back[slot, rows_of(s, PACK), :] = reply[slot, rows_of(s, PACK), :]

    last = CUT - 1

    @pl.loop(0, depth + 3)
    def _(i):
        @pl.when(i == depth + 2)
        def _():
            @pl.loop(0, depth)
            def _(k):
                target = looked_up(late, z, k)

                @pl.when(target >= 0)
                def _():
                    for p in range(HOP):
                        cols = slice(p * hop_w, (p + 1) * hop_w)
                        chain_copy(p, target, target, True).wait_recv()
                        away[target, :, cols] = (
                            parts[target, :, cols] + come[target, :, cols].astype(F32)
                        ).astype(BF16)
                        pass_on(p, target)

        @pl.when(i > 2)
        def _():
            combine((i - 2) % depth)

        @pl.when((i > 0) & (i < depth))
        def _():
            arrive(i, last)

        @pl.when(i < depth)
        def _():
            for h in range(last):

                @pl.when(i == 0)
                def _():
                    dispatch(i, h)

            dispatch(i, last)

        for k in range(2, tp, 2):

            @pl.when(i < FEED)
            def _():
                weight_far(k, t, i).start()

            @pl.when((i > 0) & (i <= FEED))
            def _():
                weight_far(k, far_owner(t, k), i - 1).wait_recv()
                weight_relay(k, far_owner(t, k), i - 1).start()
                if halves == 2:
                    weight_cross(k, far_owner(t, k), mine, i - 1).start()

            if halves == 2:

                @pl.when((i > 1) & (i <= FEED + 1))
                def _():
                    weight_cross(k, far_owner(t, k), 1 - mine, i - 2).wait_recv()
                    cross_relay(k, far_owner(t, k), i - 2).start()

        @pl.when(i == 0)
        def _():
            loads[0].wait()
            loads[1].wait()

            @pl.when(me > 0)
            def _():
                for which in range(2):
                    halo_copy(which, me - 1).wait_recv()
                for b in range(blocks):
                    cols = slice(b * LANES, (b + 1) * LANES)
                    glu[b, 0:margin, :] = halo_v[:, cols].astype(F32) * jax.nn.sigmoid(
                        halo_g[:, cols].astype(F32)
                    )

            @pl.when(me == 0)
            def _():
                for b in range(blocks):
                    glu[b, 0:margin, :] = jnp.zeros((margin, LANES), F32)

        @pl.when(i < depth)
        def _():
            conv_tile(i)

        @pl.when(i < depth - 1)
        def _():
            arrive(i + 1, CUT)
            for h in range(last):
                arrive(i + 1, h)
                dispatch(i + 1, h)

        @pl.when(i == 0)
        def _():
            for load in loads[2:]:
                load.wait()

        @pl.when(i < depth)
        def _():
            for h in range(CUT):

                @pl.loop(1, slab)
                def _(k):
                    block_copy(i, h, k, (s + slab - k) % slab, s).wait_recv()

            experts(i)

        @pl.when((i > 0) & (i <= depth))
        def _():
            send_back(i % depth)

        @pl.when(i == depth)
        def _():
            weight_own(sibling).wait_recv()

            @pl.loop(0, FEED)
            def _(c):
                for k in range(2, tp, 2):
                    weight_relay(k, far_owner(sibling, k), c).wait_recv()
                    if halves == 2:
                        cross_relay(k, far_owner(sibling, k), c).wait_recv()

            @pl.loop(0, 2 * depth)
            def _(c):
                mix(c)

    for p in range(HOP):
        cols = slice(p * hop_w, (p + 1) * hop_w)

        @pl.when(z > 0)
        def _():
            chain_copy(p, z, z, True).wait_recv()
            parts[z, :, cols] += come[z, :, cols].astype(F32)

        @pl.when(z < depth - 1)
        def _():
            chain_copy(p, z, depth, True).wait_recv()
            parts[z, :, cols] += come[depth, :, cols].astype(F32)

        moe_out[:, cols] = parts[z, :, cols].astype(BF16)

    @pl.when(me < n - 1)
    def _():
        for which in range(2):
            halo_copy(which, me + 1).wait_send()

    weight_own(t).wait_send()

    @pl.loop(0, FEED)
    def _(c):
        for k in range(2, tp, 2):
            weight_far(k, t, c).wait_send()
            weight_relay(k, far_owner(t, k), c).wait_send()
            if halves == 2:
                weight_cross(k, far_owner(t, k), mine, c).wait_send()
                cross_relay(k, far_owner(t, k), c).wait_send()

    @pl.loop(0, depth)
    def _(c):
        for part in range(CUT + 1):

            @pl.when((z < depth - 1) & (c <= z))
            def _():
                line_copy(part, c, True).wait_send()

            @pl.when((z > 0) & (c >= z))
            def _():
                line_copy(part, c, False).wait_send()

        for h in range(CUT):

            @pl.loop(1, slab)
            def _(k):
                block_copy(c, h, k, s, (s + k) % slab).wait_send()
                back_copy(c, h, k, s, (s + k) % slab).wait_send()

        @pl.when(c != z)
        def _():
            for p in range(HOP):
                chain_copy(p, c, c, True).wait_send()


ANY = pl.BlockSpec(memory_space=pl.ANY)
VMEM = pl.BlockSpec(memory_space=pltpu.VMEM)


def body(
    n,
    tp,
    glu_value,
    glu_gate,
    conv_taps,
    chan_gain,
    chan_shift,
    mix_out_weight,
    moe_input,
    moe_gain,
    expert_ids,
    expert_share,
    expert_gate_weight,
    expert_up_weight,
    expert_down_weight,
):
    tokens, per_token = expert_ids.shape
    width = moe_input.shape[1]
    sh = Shape(n, tp, tokens, per_token, width)
    slab, depth = sh.slab, sh.depth

    positions, channels = glu_value.shape
    taps_count = conv_taps.shape[0]
    margin = -(-(taps_count - 1) // PACK) * PACK
    out_width = mix_out_weight.shape[1]
    hidden_units = expert_gate_weight.shape[2]
    dma = pltpu.SemaphoreType.DMA
    packed = (depth, sh.slots, sh.pack_w)
    mixed, moe_output = pl.pallas_call(
        functools.partial(whole_kernel, sh, taps_count, margin),
        name="mixer_and_experts",
        out_shape=(
            jax.ShapeDtypeStruct((positions, out_width), BF16),
            jax.ShapeDtypeStruct((tokens, width), BF16),
        ),
        in_specs=[ANY] * 13,
        out_specs=(VMEM, VMEM),
        scratch_shapes=[
            pltpu.VMEM((depth, tokens, width), BF16),
            pltpu.VMEM((depth, sh.table_rows, sh.slots), F32),
            pltpu.VMEM(packed, BF16),
            pltpu.VMEM(packed, BF16),
            pltpu.VMEM((sh.count, width), BF16),
            pltpu.VMEM((sh.count, hidden_units), BF16),
            pltpu.VMEM((sh.count, width), BF16),
            pltpu.VMEM(packed, BF16),
            pltpu.VMEM(packed, BF16),
            pltpu.VMEM((depth + 1, tokens, width), BF16),
            pltpu.VMEM((depth, tokens, width), BF16),
            pltpu.VMEM((depth, tokens, width), F32),
            pltpu.VMEM((width, hidden_units), BF16),
            pltpu.VMEM((width, hidden_units), BF16),
            pltpu.VMEM((hidden_units, width), BF16),
            pltpu.VMEM((channels, out_width), BF16),
            pltpu.VMEM((positions, channels), BF16),
            pltpu.VMEM((positions, channels), BF16),
            pltpu.VMEM((margin, channels), BF16),
            pltpu.VMEM((margin, channels), BF16),
            pltpu.VMEM((channels // LANES, margin + positions // depth, LANES), F32),
            pltpu.VMEM((positions // depth, channels), F32),
            pltpu.VMEM((positions, channels), BF16),
            dma((depth, CUT + 1)),
            dma((depth, CUT + 1)),
            dma((depth, CUT + 1)),
            dma((depth, CUT, slab)),
            dma((depth, CUT, slab)),
            dma((depth, CUT, slab)),
            dma((depth, CUT, slab)),
            dma((depth, HOP)),
            dma((depth + 1, HOP)),
            dma((2,)),
            dma((2,)),
            dma((tp, FEED)),
            dma((tp, FEED)),
            dma((tp, FEED)),
            dma((tp, FEED)),
            dma((13,)),
            pltpu.VMEM((tokens, width), BF16),
            pltpu.VMEM((1, width), F32),
            pltpu.VMEM((per_token, tokens), jnp.int32),
            pltpu.VMEM((per_token, tokens), F32),
            pltpu.VMEM((taps_count, channels), F32),
            pltpu.VMEM((1, channels), F32),
            pltpu.VMEM((1, channels), F32),
        ],
        compiler_params=pltpu.CompilerParams(
            collective_id=0, has_side_effects=True, vmem_limit_bytes=67043328
        ),
    )(
        moe_input,
        moe_gain.reshape(1, width),
        expert_ids.T,
        expert_share.T,
        glu_value,
        glu_gate,
        conv_taps,
        chan_gain.reshape(1, channels),
        chan_shift.reshape(1, channels),
        mix_out_weight,
        expert_gate_weight,
        expert_up_weight,
        expert_down_weight,
    )
    return (mixed, moe_output)


def solution(mesh):
    tp = mesh.shape["tp"]
    n = mesh.shape["ep"] * tp
    both = P(("ep", "tp"), None)
    weights = P(("ep", "tp"), None, None)
    placed = (
        both, both, P(), P(), P(), P("tp", None), both, P(), both, both, weights, weights, weights
    )
    return jax.shard_map(
        functools.partial(body, n, tp),
        mesh=mesh,
        in_specs=placed,
        out_specs=(both, both),
        check_vma=False,
    )
```

time: 143 us -> 133 us (0.930)
  the two profiles are of different devices: /device:TPU:0 before, /device:TPU:24 now
where the time goes in v2:
time: 133 us
  Pallas kernels  127 us (95%)
  local copies, waits for them, and re-layouts  5.64 us (4%)
    pallas_call x1, Pallas kernels, body(): pl.pallas_call(functools.partial(whole_kernel, sh, taps_count, margin), n...  127 us
    unnamed x4, local copies, waits for them, and re-layouts  5.64 us

profile of v2, /device:TPU:24, one launch (start us, length us, event | category | flops | bytes accessed | tf_op | source)
XLA Modules:
  0.0 133.0 jit_solution(15457945858884867640)
XLA Ops:
  0.6 126.7 %mixer_and_experts.1 = (bf16[1024,2048]{1,0:T(8,128)(2,1)}, bf16[128,2048]{1,0:T(8,128)(2,1)}) custom-call(bf16[128,2048]{1,0:T(8,128)(2,1)} %moe.1, f32[1,2048]{1,0:T(1,128)} %bitcast.5, s32[4,128]{1,0:T(4,128)} %bitcast.8, f32[4,128]{1,0:T(4,128)} %bitcast.9, bf16[1024,1024]{1,0:T(8,128)(2,1)} %value_all.1, bf16[1024,1024]{1,0:T(8,128)(2,1)} %gate_all.1, ...), custom_call_target="tpu_custom_call" | custom-call | tf_op jit(solution)/shard_map/mixer_and_experts/pallas_call | solution.py:845
  127.4 0.0 copy-start
  127.4 4.8 %copy.17 = bf16[1024,2048]{1,0:T(8,128)(2,1)} copy(bf16[1024,2048]{1,0:T(8,128)(2,1)} %get-tuple-element.4) | data formatting | bytes 8388608
  132.2 0.0 copy-done
  132.2 0.8 copy.18
Async XLA Ops:
  127.4 4.9 %copy-start = (bf16[128,2048]{1,0:T(8,128)(2,1)S(1)}, bf16[128,2048]{1,0:T(8,128)(2,1)}, u32[]{:S(2)}) copy-start(bf16[128,2048]{1,0:T(8,128)(2,1)} %get-tuple-element.5) | copy-start | bytes 1572868

commit v3 on v2

--- a/solution.py
+++ b/solution.py
@@ -12,7 +12,7 @@
 LANES = 128
 PACK = 16
 CUT = 2
-HOP = 4
+HOP = 8
 KINDS = 4
 FEED = 2
 MESH = pl.DeviceIdType.MESH
@@ -210,6 +210,8 @@
     wu_v,
     wd_v,
     weight_v,
+    mixed_v,
+    mix_s,
     value,
     gate,
     halo_v,
@@ -232,6 +234,8 @@
     weight_r,
     cross_s,
     cross_r,
+    feed_s,
+    feed_r,
     load_s,
     moe_v,
     moe_gain_v,
@@ -348,6 +352,19 @@
             tp,
         )
 
+    fed = depth >= 3
+    at_end = ((z == 0) | (z == depth - 1)) if fed else z < 0
+    inner = jnp.logical_not(at_end)
+
+    def weight_line(k, owner, up):
+        here = weight_v.at[rows_of(owner, shard)]
+        flat = me + (slab if up else -slab)
+        return remote(here, here, feed_s.at[k + (tp if up else 0)], feed_r.at[k], flat, tp)
+
+    def line_relay(k, owner):
+        here = weight_v.at[rows_of(owner, shard)]
+        return remote(here, here, feed_s.at[k + 1], feed_r.at[k + 1], e * tp + sibling, tp)
+
     def far_owner(base, k):
         return (base + tp - k) % tp
 
@@ -604,12 +621,17 @@
     out_step = min(512, out_w)
     mix_rows = positions // (2 * depth)
 
+    def mixed_copy(c):
+        here = rows_of(c, mix_rows)
+        return pltpu.make_async_copy(mixed_v.at[here], mixed.at[here], mix_s.at[c])
+
     def mix(c):
         for f in range(out_w // out_step):
             cols = slice(f * out_step, (f + 1) * out_step)
-            mixed[rows_of(c, mix_rows), cols] = jnp.dot(
+            mixed_v[rows_of(c, mix_rows), cols] = jnp.dot(
                 act[rows_of(c, mix_rows), :], weight_v[:, cols], preferred_element_type=F32
             ).astype(BF16)
+        mixed_copy(c).start()
 
     def dispatch(slot, h):
         pack_rows(slot, h, looked_up(order, z, slot))
@@ -670,11 +692,11 @@
 
         for k in range(2, tp, 2):
 
-            @pl.when(i < FEED)
+            @pl.when(inner & (i < FEED))
             def _():
                 weight_far(k, t, i).start()
 
-            @pl.when((i > 0) & (i <= FEED))
+            @pl.when(inner & (i > 0) & (i <= FEED))
             def _():
                 weight_far(k, far_owner(t, k), i - 1).wait_recv()
                 weight_relay(k, far_owner(t, k), i - 1).start()
@@ -683,10 +705,25 @@
 
             if halves == 2:
 
-                @pl.when((i > 1) & (i <= FEED + 1))
+                @pl.when(inner & (i > 1) & (i <= FEED + 1))
                 def _():
                     weight_cross(k, far_owner(t, k), 1 - mine, i - 2).wait_recv()
                     cross_relay(k, far_owner(t, k), i - 2).start()
+
+            if fed:
+
+                @pl.when((i == FEED + 1) & (z == 1))
+                def _():
+                    weight_line(k, far_owner(t, k), False).start()
+
+                @pl.when((i == FEED + 1) & (z == depth - 2))
+                def _():
+                    weight_line(k, far_owner(t, k), True).start()
+
+                @pl.when((i == depth + 1) & at_end)
+                def _():
+                    weight_line(k, far_owner(t, k), False).wait_recv()
+                    line_relay(k, far_owner(t, k)).start()
 
         @pl.when(i == 0)
         def _():
@@ -738,16 +775,23 @@
         def _():
             send_back(i % depth)
 
-        @pl.when(i == depth)
+        @pl.when((inner & (i == depth)) | (at_end & (i == depth + 2)))
         def _():
             weight_own(sibling).wait_recv()
-
-            @pl.loop(0, FEED)
-            def _(c):
-                for k in range(2, tp, 2):
-                    weight_relay(k, far_owner(sibling, k), c).wait_recv()
-                    if halves == 2:
-                        cross_relay(k, far_owner(sibling, k), c).wait_recv()
+            for k in range(2, tp, 2):
+
+                @pl.when(inner)
+                def _():
+                    for c in range(FEED):
+                        weight_relay(k, far_owner(sibling, k), c).wait_recv()
+                        if halves == 2:
+                            cross_relay(k, far_owner(sibling, k), c).wait_recv()
+
+                if fed:
+
+                    @pl.when(at_end)
+                    def _():
+                        line_relay(k, far_owner(sibling, k)).wait_recv()
 
             @pl.loop(0, 2 * depth)
             def _(c):
@@ -775,14 +819,34 @@
 
     weight_own(t).wait_send()
 
-    @pl.loop(0, FEED)
+    @pl.loop(0, 2 * depth)
     def _(c):
-        for k in range(2, tp, 2):
-            weight_far(k, t, c).wait_send()
-            weight_relay(k, far_owner(t, k), c).wait_send()
-            if halves == 2:
-                weight_cross(k, far_owner(t, k), mine, c).wait_send()
-                cross_relay(k, far_owner(t, k), c).wait_send()
+        mixed_copy(c).wait()
+
+    for k in range(2, tp, 2):
+
+        @pl.when(inner)
+        def _():
+            for c in range(FEED):
+                weight_far(k, t, c).wait_send()
+                weight_relay(k, far_owner(t, k), c).wait_send()
+                if halves == 2:
+                    weight_cross(k, far_owner(t, k), mine, c).wait_send()
+                    cross_relay(k, far_owner(t, k), c).wait_send()
+
+        if fed:
+
+            @pl.when(at_end)
+            def _():
+                line_relay(k, far_owner(t, k)).wait_send()
+
+            @pl.when(z == 1)
+            def _():
+                weight_line(k, far_owner(t, k), False).wait_send()
+
+            @pl.when(z == depth - 2)
+            def _():
+                weight_line(k, far_owner(t, k), True).wait_send()
 
     @pl.loop(0, depth)
     def _(c):
@@ -850,7 +914,7 @@
             jax.ShapeDtypeStruct((tokens, width), BF16),
         ),
         in_specs=[ANY] * 13,
-        out_specs=(VMEM, VMEM),
+        out_specs=(ANY, VMEM),
         scratch_shapes=[
             pltpu.VMEM((depth, tokens, width), BF16),
             pltpu.VMEM((depth, sh.table_rows, sh.slots), F32),
@@ -868,6 +932,8 @@
             pltpu.VMEM((width, hidden_units), BF16),
             pltpu.VMEM((hidden_units, width), BF16),
             pltpu.VMEM((channels, out_width), BF16),
+            pltpu.VMEM((positions, out_width), BF16),
+            dma((2 * depth,)),
             pltpu.VMEM((positions, channels), BF16),
             pltpu.VMEM((positions, channels), BF16),
             pltpu.VMEM((margin, channels), BF16),
@@ -890,6 +956,8 @@
             dma((tp, FEED)),
             dma((tp, FEED)),
             dma((tp, FEED)),
+            dma((2 * tp,)),
+            dma((tp,)),
             dma((13,)),
             pltpu.VMEM((tokens, width), BF16),
             pltpu.VMEM((1, width), F32),

time: 133 us -> 131 us (0.985)
  Pallas kernels: 127 us -> 125 us
    pallas_call x1, Pallas kernels: 127 us -> 125 us  [body(): pl.pallas_call(functools.partial(whole_kernel, sh, taps_count, margin), n...]
where the time goes in v3:
time: 131 us
  Pallas kernels  125 us (95%)
  local copies, waits for them, and re-layouts  5.64 us (4%)
    pallas_call x1, Pallas kernels, body(): pl.pallas_call(functools.partial(whole_kernel, sh, taps_count, margin), n...  125 us
    unnamed x4, local copies, waits for them, and re-layouts  5.64 us

profile of v3, /device:TPU:24, one launch (start us, length us, event | category | flops | bytes accessed | tf_op | source)
XLA Modules:
  0.0 131.3 jit_solution(8205839495499935272)
XLA Ops:
  0.6 125.0 %mixer_and_experts.1 = (bf16[1024,2048]{1,0:T(8,128)(2,1)}, bf16[128,2048]{1,0:T(8,128)(2,1)}) custom-call(bf16[128,2048]{1,0:T(8,128)(2,1)} %moe.1, f32[1,2048]{1,0:T(1,128)} %bitcast.5, s32[4,128]{1,0:T(4,128)} %bitcast.8, f32[4,128]{1,0:T(4,128)} %bitcast.9, bf16[1024,1024]{1,0:T(8,128)(2,1)} %value_all.1, bf16[1024,1024]{1,0:T(8,128)(2,1)} %gate_all.1, ...), custom_call_target="tpu_custom_call" | custom-call | tf_op jit(solution)/shard_map/mixer_and_experts/pallas_call | solution.py:909
  125.6 0.0 copy-start
  125.6 4.8 %copy.17 = bf16[1024,2048]{1,0:T(8,128)(2,1)} copy(bf16[1024,2048]{1,0:T(8,128)(2,1)} %get-tuple-element.4) | data formatting | bytes 8388608
  130.5 0.0 copy-done
  130.5 0.8 copy.18
Async XLA Ops:
  125.6 4.9 %copy-start = (bf16[128,2048]{1,0:T(8,128)(2,1)S(1)}, bf16[128,2048]{1,0:T(8,128)(2,1)}, u32[]{:S(2)}) copy-start(bf16[128,2048]{1,0:T(8,128)(2,1)} %get-tuple-element.5) | copy-start | bytes 1572868
